TPU v7x, 32 devices: a whole 2x2x4 slice. The times are simulated.
32 devices in a mesh: rep: 2 (over x), fs: 4 (over z), tp: 4 (over y, core).
Axes of the slice: x: 2, y: 2, z: 4, core: 2. Of those that a mesh axis runs over, the one named last changes fastest.
Arguments:
- tokens: bfloat16 [4096, 2048], P(('rep', 'fs', 'tp')), may hold values from -6 to 6
- mix_gain: float32 [2048], replicated, may hold values from 0.1 to 1.9
- w_query: bfloat16 [2048, 1024], P('fs', 'tp'), may hold values from -0.125 to 0.125
- w_key: bfloat16 [2048, 1024], P('fs', 'tp'), may hold values from -0.125 to 0.125
- w_value: bfloat16 [2048, 2048], P('fs', 'tp'), may hold values from -0.125 to 0.125
- w_decay_down: bfloat16 [2048, 32], replicated, may hold values from -0.125 to 0.125
- w_decay_up: bfloat16 [32, 1024], replicated, may hold values from -2 to 2
- decay_bias: float32 [1024], replicated, may hold values from -1 to 6
- decay_shift: float32 [4096, 1024], P(('rep', 'fs'), 'tp'), may hold values from -3 to 0
- head_gain: float32 [2048], replicated, may hold values from 0.1 to 1.9
- w_mix_out: bfloat16 [2048, 2048], P('tp', 'fs'), may hold values from -0.125 to 0.125
- ffn_gain: float32 [2048], replicated, may hold values from 0.1 to 1.9
- w_gate: bfloat16 [2048, 5632], P('fs', 'tp'), may hold values from -0.125 to 0.125
- w_up: bfloat16 [2048, 5632], P('fs', 'tp'), may hold values from -0.125 to 0.125
- w_down: bfloat16 [5632, 2048], P('tp', 'fs'), may hold values from -0.078125 to 0.078125
Outputs:
- layer_out: float32 [4096, 2048], P(('rep', 'fs', 'tp'))
All inputs are finite; a program needn't handle non-finite values.
Results may differ from a plain program's by a relative error of at most 0.04.
Values may be sent and summed in bfloat16 or wider, within the bound.
A program may use at most 128 MiB of HBM per device.

v0:
```python
import jax
import jax.numpy as jnp
from jax import lax
from jax.sharding import PartitionSpec as P

KEY_CHANNELS = 128
DV = 256
BLK = 64


EPS = 1e-06
TAU = 16.0


def rms_norm(values, gain):
    return values * lax.rsqrt(jnp.mean(values * values, axis=-1, keepdims=True) + EPS) * gain


def recurrence(query_proj, key_proj, value_proj, log_decay, head_count):
    seq_rows = query_proj.shape[0]
    blocks = seq_rows // BLK
    exact = lax.Precision.HIGHEST
    queries = query_proj.astype(jnp.float32).reshape(
        blocks, BLK, head_count, KEY_CHANNELS
    ) * KEY_CHANNELS ** (-0.5)
    keys = key_proj.astype(jnp.float32).reshape(blocks, BLK, head_count, KEY_CHANNELS)
    values = value_proj.astype(jnp.float32).reshape(blocks, BLK, head_count, DV)
    decays = log_decay.reshape(blocks, BLK, head_count, KEY_CHANNELS)
    lower = (jnp.arange(BLK)[:, None] >= jnp.arange(BLK)[None, :]).astype(jnp.float32)
    cumul = jnp.einsum("cs,bshd->bchd", lower, decays, precision=exact)
    totals = cumul[:, -1]
    weighted = keys * jnp.exp(totals[:, None] - cumul)
    updates = jnp.einsum("bchd,bche->bhde", weighted, values, precision=exact)
    state = jnp.zeros_like(updates[0])
    previous = []
    for block in range(blocks):
        previous.append(state)
        state = jnp.exp(totals[block])[..., None] * state + updates[block]
    previous = jnp.stack(previous)
    q_decayed = queries * jnp.exp(cumul)
    k_decayed = keys * jnp.exp(-cumul)
    scores = jnp.einsum("bchd,bshd->bhcs", q_decayed, k_decayed, precision=exact)
    scores = scores * lower
    inner = jnp.einsum("bhcs,bshe->bche", scores, values, precision=exact)
    carried = jnp.einsum("bchd,bhde->bche", q_decayed, previous, precision=exact)
    return (inner + carried).reshape(seq_rows, head_count, DV)


def shift(values, axis, distance):
    count = lax.axis_size(axis)
    return lax.ppermute(values, axis, [(i, (i + distance) % count) for i in range(count)])


def swap_core(values):
    return lax.ppermute(values, "tp", [(i, i ^ 1) for i in range(lax.axis_size("tp"))])


def gather_rows(block):
    count = lax.axis_size("tp")
    index = lax.axis_index("tp")
    chips, core, chip = count // 2, index % 2, index // 2
    rows = block.shape[0]
    mine = [block] + [shift(block, "tp", 2 * k) for k in range(1, chips)]
    whole = jnp.zeros((count * rows,) + block.shape[1:], block.dtype)
    for k, piece in enumerate(mine):
        source = (chip - k) % chips
        theirs = swap_core(piece)
        whole = lax.dynamic_update_slice_in_dim(whole, piece, (2 * source + core) * rows, 0)
        whole = lax.dynamic_update_slice_in_dim(whole, theirs, (2 * source + 1 - core) * rows, 0)
    return whole


def scatter_sum(partial):
    count = lax.axis_size("tp")
    index = lax.axis_index("tp")
    chips, core, chip = count // 2, index % 2, index // 2
    rows = partial.shape[0] // count
    blocks = partial.astype(jnp.bfloat16).reshape(chips, 2, rows, partial.shape[1])
    away = lax.dynamic_index_in_dim(blocks, 1 - core, 1, keepdims=False)
    kept = lax.dynamic_index_in_dim(blocks, core, 1, keepdims=False).astype(jnp.float32)
    pair = kept + swap_core(away).astype(jnp.float32)
    rounded = pair.astype(jnp.bfloat16)
    total = lax.dynamic_index_in_dim(pair, chip, 0, keepdims=False)
    for k in range(1, chips):
        outgoing = lax.dynamic_index_in_dim(rounded, (chip + k) % chips, 0, keepdims=False)
        total = total + shift(outgoing, "tp", 2 * k).astype(jnp.float32)
    return total


def row_parts(weight):
    reps = lax.axis_size("rep")
    share = weight.shape[0] // reps
    own = lax.dynamic_slice_in_dim(weight, lax.axis_index("rep") * share, share, 0)
    own = lax.all_gather(own, "fs", axis=0, tiled=True)
    return [own] + [shift(own, "rep", k) for k in range(1, reps)]


def column_parts(weight):
    reps = lax.axis_size("rep")
    share = weight.shape[1] // reps
    own = lax.dynamic_slice_in_dim(weight, lax.axis_index("rep") * share, share, 1)
    own = lax.all_gather(own, "fs", axis=0, tiled=False)
    return [own] + [shift(own, "rep", k) for k in range(1, reps)]


def input_parts(values):
    reps, groups = lax.axis_size("rep"), lax.axis_size("fs")
    share = values.shape[1] // (reps * groups)
    layouts = [
        jnp.concatenate(
            [
                values[:, (g * reps + j) * share : (g * reps + j + 1) * share]
                for g in range(groups)
            ],
            axis=1,
        )
        for j in range(reps)
    ]
    index = lax.axis_index("rep")
    return [
        lax.select_n(jnp.full((), (index - k) % reps, jnp.int32), *layouts) if reps > 2
        else (jnp.where((index - k) % reps == 0, layouts[0], layouts[-1]))
        for k in range(reps)
    ]


def dots(inputs, weights):
    total = jnp.dot(inputs[0], weights[0], preferred_element_type=jnp.float32)
    for left, right in zip(inputs[1:], weights[1:]):
        total = total + jnp.dot(left, right, preferred_element_type=jnp.float32)
    return total


def project_out(values, weights):
    reps = lax.axis_size("rep")
    index = lax.axis_index("rep")
    sums = []
    for weight in weights:
        partial = jnp.concatenate(
            [
                jnp.dot(values, weight[g], preferred_element_type=jnp.float32)
                for g in range(weight.shape[0])
            ],
            axis=1,
        )
        sums.append(scatter_sum(partial))
    share = weights[0].shape[2]
    ordered = []
    for j in range(reps):
        if reps == 2:
            ordered.append(jnp.where(index == j, sums[0], sums[1]))
        else:
            ordered.append(lax.select_n((index - j) % reps, *sums))
    pieces = []
    for g in range(weights[0].shape[0]):
        for j in range(reps):
            pieces.append(ordered[j][:, g * share : (g + 1) * share])
    return jnp.concatenate(pieces, axis=1)


def per_device(
    tokens,
    mix_gain,
    w_query,
    w_key,
    w_value,
    w_decay_down,
    w_decay_up,
    decay_bias,
    decay_shift,
    head_gain,
    w_mix_out,
    ffn_gain,
    w_gate,
    w_up,
    w_down,
):
    tp_index = lax.axis_index("tp")
    key_cols = w_query.shape[1]
    value_cols = w_value.shape[1]
    heads_dev = key_cols // KEY_CHANNELS
    own_tokens = tokens.astype(jnp.float32)
    qkv_weights = row_parts(jnp.concatenate([w_query, w_key, w_value], axis=1))
    out_weights = column_parts(w_mix_out)
    gate_weights = row_parts(w_gate)
    up_weights = row_parts(w_up)
    down_weights = column_parts(w_down)
    normed = gather_rows(rms_norm(own_tokens, mix_gain).astype(jnp.bfloat16))
    seq_rows = normed.shape[0]
    low_rank = jnp.dot(normed, w_decay_down, preferred_element_type=jnp.float32).astype(
        jnp.bfloat16
    )
    up_columns = lax.dynamic_slice_in_dim(w_decay_up, tp_index * key_cols, key_cols, 1)
    bias_columns = lax.dynamic_slice_in_dim(decay_bias, tp_index * key_cols, key_cols, 0)
    pre_decay = jnp.dot(low_rank, up_columns, preferred_element_type=jnp.float32) + bias_columns
    log_decay = jax.nn.log_sigmoid(pre_decay) / TAU + decay_shift
    projected = dots(input_parts(normed), qkv_weights).astype(jnp.bfloat16)
    query_proj = projected[:, :key_cols]
    key_proj = projected[:, key_cols : 2 * key_cols]
    value_proj = projected[:, 2 * key_cols :]
    head_out = recurrence(query_proj, key_proj, value_proj, log_decay, heads_dev)
    gain_columns = lax.dynamic_slice_in_dim(head_gain, tp_index * value_cols, value_cols, 0)
    gated = rms_norm(head_out, gain_columns.reshape(heads_dev, DV)).astype(jnp.bfloat16)
    gated = gated.reshape(seq_rows, value_cols)
    hidden = own_tokens + project_out(gated, out_weights)
    normed_ffn = gather_rows(rms_norm(hidden, ffn_gain).astype(jnp.bfloat16))
    ffn_inputs = input_parts(normed_ffn)
    gate_proj = dots(ffn_inputs, gate_weights)
    up_proj = dots(ffn_inputs, up_weights)
    activated = (jax.nn.silu(gate_proj) * up_proj).astype(jnp.bfloat16)
    return hidden + project_out(activated, down_weights)


def solution(mesh):
    return jax.shard_map(
        per_device,
        mesh=mesh,
        in_specs=(
            P(("rep", "fs", "tp"), None),
            P(),
            P("fs", "tp"),
            P("fs", "tp"),
            P("fs", "tp"),
            P(),
            P(),
            P(),
            P(("rep", "fs"), "tp"),
            P(),
            P("tp", "fs"),
            P(),
            P("fs", "tp"),
            P("fs", "tp"),
            P("tp", "fs"),
        ),
        out_specs=P(("rep", "fs", "tp"), None),
        check_vma=False,
    )
```

profile of v0, /device:TPU:0, one launch (start us, length us, event | category | flops | bytes accessed | tf_op | source)
XLA Modules:
  0.0 363.5 jit_solution(11407254583215100104)
XLA Ops:
  6.5 2.1 fusion.13
  13.4 3.0 collective-permute-start.1
  18.1 10.2 %collective-permute-done.1 = bf16[128,2048]{1,0:T(8,128)(2,1)S(1)} collective-permute-done((bf16[128,2048]{1,0:T(8,128)(2,1)S(1)}, bf16[128,2048]{1,0:T(8,128)(2,1)S(1)}, u32[]{:S(2)}, u32[]{:S(2)}) %collective-permute-start.1) | collective-permute-done | bytes 524320 | tf_op jit(solution)/shard_map/ppermute | solution.py:51
  29.9 27.4 %all-gather.8.cloned.1.call-done = bf16[1024,1024]{1,0:T(8,128)(2,1)} async-done(((bf16[256,1024]{1,0:T(8,128)(2,1)}), bf16[1024,1024]{1,0:T(8,128)(2,1)}) %all-gather.8.cloned.1.call-update) | async-done | bytes 2097168 | tf_op jit(solution)/shard_map/all_gather | solution.py:94
  61.3 2.7 fusion.16
  64.8 1.8 fusion.56
  66.5 19.2 %all-gather.14.cloned.1.call-done = bf16[2048,256]{1,0:T(8,128)(2,1)} async-done(((bf16[512,256]{1,0:T(8,128)(2,1)}), bf16[2048,256]{1,0:T(8,128)(2,1)}) %all-gather.14.cloned.1.call-update) | async-done | bytes 1048592 | tf_op jit(solution)/shard_map/all_gather | solution.py:102
  87.2 2.8 fusion.8
  90.0 16.1 %collective-permute-done.3 = bf16[1024,1024]{1,0:T(8,128)(2,1)} collective-permute-done((bf16[1024,1024]{1,0:T(8,128)(2,1)}, bf16[1024,1024]{1,0:T(8,128)(2,1)}, u32[]{:S(2)}, u32[]{:S(2)}) %collective-permute-start.3) | collective-permute-done | bytes 2097184 | tf_op jit(solution)/shard_map/ppermute | solution.py:51
  106.1 2.9 add_convert_fusion
  117.9 9.5 %collective-permute-done.6 = bf16[4,512,256]{2,1,0:T(8,128)(2,1)} collective-permute-done((bf16[4,512,256]{2,1,0:T(8,128)(2,1)}, bf16[4,512,256]{2,1,0:T(8,128)(2,1)}, u32[]{:S(2)}, u32[]{:S(2)}) %collective-permute-start.6) | collective-permute-done | bytes 1048608 | tf_op jit(solution)/shard_map/ppermute | solution.py:51
  141.0 4.8 %all-gather.10.cloned.1.call-done = bf16[1024,1408]{1,0:T(8,128)(2,1)} async-done(((bf16[256,1408]{1,0:T(8,128)(2,1)}), bf16[1024,1408]{1,0:T(8,128)(2,1)}) %all-gather.10.cloned.1.call-update) | async-done | bytes 2883600 | tf_op jit(solution)/shard_map/all_gather | solution.py:94
  147.3 4.2 %collective-permute-done.5 = bf16[128,1024]{1,0:T(8,128)(2,1)S(1)} collective-permute-done((bf16[128,1024]{1,0:T(8,128)(2,1)S(1)}, bf16[128,1024]{1,0:T(8,128)(2,1)S(1)}, u32[]{:S(2)}, u32[]{:S(2)}) %collective-permute-start.5) | collective-permute-done | bytes 262176 | tf_op jit(solution)/shard_map/ppermute | solution.py:51
  157.1 47.9 %all-gather.12.cloned.1.call-done = bf16[1024,1408]{1,0:T(8,128)(2,1)} async-done(((bf16[256,1408]{1,0:T(8,128)(2,1)}), bf16[1024,1408]{1,0:T(8,128)(2,1)}) %all-gather.12.cloned.1.call-update) | async-done | bytes 2883600 | tf_op jit(solution)/shard_map/all_gather | solution.py:94
  206.5 57.8 %all-gather.16.cloned.1.call-done = bf16[5632,256]{1,0:T(8,128)(2,1)} async-done(((bf16[1408,256]{1,0:T(8,128)(2,1)}), bf16[5632,256]{1,0:T(8,128)(2,1)}) %all-gather.16.cloned.1.call-update) | async-done | bytes 2883600 | tf_op jit(solution)/shard_map/all_gather | solution.py:102
  267.5 1.9 constant_dynamic-update-slice_fusion.3
  269.4 1.8 fusion.55
  271.8 1.8 fusion.32
  273.7 1.8 fusion.31
  275.5 3.6 %convolution_add_fusion.1 = f32[512,1408]{1,0:T(8,128)S(1)} fusion(f32[512,1408]{1,0:T(8,128)S(1)} %fusion.32, bf16[1024,1408]{1,0:T(8,128)(2,1)} %collective-permute-done.12, pred[]{:T(512)S(6)} %eq.37, bf16[512,256]{1,0:T(8,128)(2,1)S(1)} %get-tuple-element.20, bf16[512,256]{1,0:T(8,128)(2,1)S(1)} %get-tuple-element.21, ...), kind=kOutput, calls=%fused_computation.2 | convolution fusion | flops 1486028800 | bytes 10747905 | tf_op jit(solution)/shard_map/dot_general | solution.py:130
  279.2 4.4 %fusion.1 = bf16[512,1408]{1,0:T(8,128)(2,1)S(1)} fusion(f32[512,1408]{1,0:T(8,128)S(1)} %fusion.31, bf16[1024,1408]{1,0:T(8,128)(2,1)} %collective-permute-done.13, f32[512,1408]{1,0:T(8,128)S(1)} %convolution_add_fusion.1, pred[]{:T(512)S(6)} %eq.37, bf16[512,256]{1,0:T(8,128)(2,1)S(1)} %get-tuple-element.20, bf16[512,256]{1,0:T(8,128)(2,1)S(1)} %get-tuple-element.21, ...), kind=kOutput, calls=%fused_computation.3 | convolution fusion | flops 1490354176 | bytes 12189697 | tf_op jit(solution)/shard_map/dot_general | solution.py:130
  283.5 50.1 %collective-permute-done.16 = bf16[4,1408,256]{2,1,0:T(8,128)(2,1)S(1)} collective-permute-done((bf16[4,1408,256]{2,1,0:T(8,128)(2,1)}, bf16[4,1408,256]{2,1,0:T(8,128)(2,1)S(1)}, u32[]{:S(2)}, u32[]{:S(2)}) %collective-permute-start.16) | collective-permute-done | bytes 2883616 | tf_op jit(solution)/shard_map/ppermute | solution.py:51
  344.0 5.8 %collective-permute-done.18 = bf16[128,1024]{1,0:T(8,128)(2,1)S(1)} collective-permute-done((bf16[128,1024]{1,0:T(8,128)(2,1)S(1)}, bf16[128,1024]{1,0:T(8,128)(2,1)S(1)}, u32[]{:S(2)}, u32[]{:S(2)}) %collective-permute-start.18) | collective-permute-done | bytes 262176 | tf_op jit(solution)/shard_map/ppermute | solution.py:51
  349.8 5.1 %collective-permute-done.15 = bf16[128,1024]{1,0:T(8,128)(2,1)S(1)} collective-permute-done((bf16[128,1024]{1,0:T(8,128)(2,1)S(1)}, bf16[128,1024]{1,0:T(8,128)(2,1)S(1)}, u32[]{:S(2)}, u32[]{:S(2)}) %collective-permute-start.15) | collective-permute-done | bytes 262176 | tf_op jit(solution)/shard_map/ppermute | solution.py:51
  (173 shorter events, 60.7 us)
Async XLA Ops:
  6.5 50.8 %all-gather.8.cloned.1.call-start = ((), (), s32[]{:S(2)}) async-start(), calls=%async_computation | async-start | bytes 2621440 | tf_op jit(solution)/shard_map/all_gather | solution.py:94
  8.6 77.1 %all-gather.14.cloned.1.call-start = ((), (), s32[]{:S(2)}) async-start(), calls=%async_computation.3 | async-start | bytes 1310720 | tf_op jit(solution)/shard_map/all_gather | solution.py:102
  9.4 136.4 %all-gather.10.cloned.1.call-start = ((), (), s32[]{:S(2)}) async-start(), calls=%async_computation.1 | async-start | bytes 3604480 | tf_op jit(solution)/shard_map/all_gather | solution.py:94
  10.5 194.6 %all-gather.12.cloned.1.call-start = ((), (), s32[]{:S(2)}) async-start(), calls=%async_computation.2 | async-start | bytes 3604480 | tf_op jit(solution)/shard_map/all_gather | solution.py:94
  13.4 14.9 %collective-permute-start.1 = (bf16[128,2048]{1,0:T(8,128)(2,1)S(1)}, bf16[128,2048]{1,0:T(8,128)(2,1)S(1)}, u32[]{:S(2)}, u32[]{:S(2)}) collective-permute-start(bf16[128,2048]{1,0:T(8,128)(2,1)S(1)} %get-tuple-element.14), channel_id=1, source_target_pairs={{0,2},{1,3},{2,0},{3,1},{4,6},{5,7},{6,4},{7,5},{8,10},{9,11},{10,... | collective-permute-start | bytes 1572872 | tf_op jit(solution)/shard_map/ppermute | solution.py:51
  16.4 42.4 %collective-permute-start = (bf16[128,2048]{1,0:T(8,128)(2,1)S(1)}, bf16[128,2048]{1,0:T(8,128)(2,1)S(1)}, u32[]{:S(2)}, u32[]{:S(2)}) collective-permute-start(bf16[128,2048]{1,0:T(8,128)(2,1)S(1)} %get-tuple-element.14), channel_id=1, source_target_pairs={{0,1},{1,0},{2,3},{3,2},{4,5},{5,4},{6,7},{7,6},{8,9},{9,8},{10,11... | collective-permute-start | bytes 1572872 | tf_op jit(solution)/shard_map/ppermute | solution.py:55
  17.3 247.0 %all-gather.16.cloned.1.call-start = ((), (), s32[]{:S(2)}) async-start(), calls=%async_computation.4 | async-start | bytes 3604480 | tf_op jit(solution)/shard_map/all_gather | solution.py:102
  28.3 32.2 %collective-permute-start.2 = (bf16[128,2048]{1,0:T(8,128)(2,1)S(1)}, bf16[128,2048]{1,0:T(8,128)(2,1)S(1)}, u32[]{:S(2)}, u32[]{:S(2)}) collective-permute-start(bf16[128,2048]{1,0:T(8,128)(2,1)S(1)} %collective-permute-done.1), channel_id=1, source_target_pairs={{0,1},{1,0},{2,3},{3,2},{4,5},{5,4},{6,7},{7,6},{8,9},{9,8},{10,11... | collective-permute-start | bytes 1572872 | tf_op jit(solution)/shard_map/ppermute | solution.py:55
  57.3 48.8 %collective-permute-start.3 = (bf16[1024,1024]{1,0:T(8,128)(2,1)}, bf16[1024,1024]{1,0:T(8,128)(2,1)}, u32[]{:S(2)}, u32[]{:S(2)}) collective-permute-start(bf16[1024,1024]{1,0:T(8,128)(2,1)} %all-gather.8.cloned.1.call-done), channel_id=1, source_target_pairs={{0,16},{16,0},{1,17},{17,1},{2,18},{18,2},{3,19},{19,3},{4,20},{20... | collective-permute-start | bytes 6291464 | tf_op jit(solution)/shard_map/ppermute | solution.py:51
  85.7 41.6 %collective-permute-start.6 = (bf16[4,512,256]{2,1,0:T(8,128)(2,1)}, bf16[4,512,256]{2,1,0:T(8,128)(2,1)}, u32[]{:S(2)}, u32[]{:S(2)}) collective-permute-start(bf16[4,512,256]{2,1,0:T(8,128)(2,1)} %bitcast.206), channel_id=1, source_target_pairs={{0,16},{16,0},{1,17},{17,1},{2,18},{18,2},{3,19},{19,3},{4,20},{20... | collective-permute-start | bytes 3145736 | tf_op jit(solution)/shard_map/ppermute | solution.py:51
  133.4 3.9 %collective-permute-start.7 = (bf16[2,128,1024]{2,1,0:T(8,128)(2,1)}, bf16[2,128,1024]{2,1,0:T(8,128)(2,1)S(1)}, u32[]{:S(2)}, u32[]{:S(2)}) collective-permute-start(bf16[2,128,1024]{2,1,0:T(8,128)(2,1)} %dynamic-slice_bitcast_fusion.2), channel_id=1, source_target_pairs={{0,1},{1,0},{2,3},{3,2},{4,5},{5,4},{6,7},{7,6},{8,9},{9,8},{10,11... | collective-permute-start | bytes 1572872 | tf_op jit(solution)/shard_map/ppermute | solution.py:55
  135.8 3.3 collective-permute-start.4
  137.5 9.7 %collective-permute-start.8 = (bf16[128,1024]{1,0:T(8,128)(2,1)S(1)}, bf16[128,1024]{1,0:T(8,128)(2,1)S(1)}, u32[]{:S(2)}, u32[]{:S(2)}) collective-permute-start(bf16[128,1024]{1,0:T(8,128)(2,1)S(1)} %fusion.38), channel_id=1, source_target_pairs={{0,2},{1,3},{2,0},{3,1},{4,6},{5,7},{6,4},{7,5},{8,10},{9,11},{10,... | collective-permute-start | bytes 786440 | tf_op jit(solution)/shard_map/ppermute | solution.py:51
  140.3 11.2 %collective-permute-start.5 = (bf16[128,1024]{1,0:T(8,128)(2,1)S(1)}, bf16[128,1024]{1,0:T(8,128)(2,1)S(1)}, u32[]{:S(2)}, u32[]{:S(2)}) collective-permute-start(bf16[128,1024]{1,0:T(8,128)(2,1)S(1)} %fusion.37), channel_id=1, source_target_pairs={{0,2},{1,3},{2,0},{3,1},{4,6},{5,7},{6,4},{7,5},{8,10},{9,11},{10,... | collective-permute-start | bytes 786440 | tf_op jit(solution)/shard_map/ppermute | solution.py:51
  145.8 129.7 %collective-permute-start.12 = (bf16[1024,1408]{1,0:T(8,128)(2,1)}, bf16[1024,1408]{1,0:T(8,128)(2,1)}, u32[]{:S(2)}, u32[]{:S(2)}) collective-permute-start(bf16[1024,1408]{1,0:T(8,128)(2,1)} %all-gather.10.cloned.1.call-done), channel_id=1, source_target_pairs={{0,16},{16,0},{1,17},{17,1},{2,18},{18,2},{3,19},{19,3},{4,20},{20... | collective-permute-start | bytes 8650760 | tf_op jit(solution)/shard_map/ppermute | solution.py:51
  155.7 50.9 %collective-permute-start.10 = (bf16[128,2048]{1,0:T(8,128)(2,1)S(1)}, bf16[128,2048]{1,0:T(8,128)(2,1)S(1)}, u32[]{:S(2)}, u32[]{:S(2)}) collective-permute-start(bf16[128,2048]{1,0:T(8,128)(2,1)S(1)} %get-tuple-element.6), channel_id=1, source_target_pairs={{0,2},{1,3},{2,0},{3,1},{4,6},{5,7},{6,4},{7,5},{8,10},{9,11},{10,... | collective-permute-start | bytes 1572872 | tf_op jit(solution)/shard_map/ppermute | solution.py:51
  157.1 108.7 %collective-permute-start.9 = (bf16[128,2048]{1,0:T(8,128)(2,1)S(1)}, bf16[128,2048]{1,0:T(8,128)(2,1)S(1)}, u32[]{:S(2)}, u32[]{:S(2)}) collective-permute-start(bf16[128,2048]{1,0:T(8,128)(2,1)S(1)} %get-tuple-element.6), channel_id=1, source_target_pairs={{0,1},{1,0},{2,3},{3,2},{4,5},{5,4},{6,7},{7,6},{8,9},{9,8},{10,11... | collective-permute-start | bytes 1572872 | tf_op jit(solution)/shard_map/ppermute | solution.py:55
  205.1 74.1 %collective-permute-start.13 = (bf16[1024,1408]{1,0:T(8,128)(2,1)}, bf16[1024,1408]{1,0:T(8,128)(2,1)}, u32[]{:S(2)}, u32[]{:S(2)}) collective-permute-start(bf16[1024,1408]{1,0:T(8,128)(2,1)} %all-gather.12.cloned.1.call-done), channel_id=1, source_target_pairs={{0,16},{16,0},{1,17},{17,1},{2,18},{18,2},{3,19},{19,3},{4,20},{20... | collective-permute-start | bytes 8650760 | tf_op jit(solution)/shard_map/ppermute | solution.py:51
  206.5 60.9 %collective-permute-start.11 = (bf16[128,2048]{1,0:T(8,128)(2,1)S(1)}, bf16[128,2048]{1,0:T(8,128)(2,1)}, u32[]{:S(2)}, u32[]{:S(2)}) collective-permute-start(bf16[128,2048]{1,0:T(8,128)(2,1)S(1)} %collective-permute-done.10), channel_id=1, source_target_pairs={{0,1},{1,0},{2,3},{3,2},{4,5},{5,4},{6,7},{7,6},{8,9},{9,8},{10,11... | collective-permute-start | bytes 1572872 | tf_op jit(solution)/shard_map/ppermute | solution.py:55
  264.3 69.4 %collective-permute-start.16 = (bf16[4,1408,256]{2,1,0:T(8,128)(2,1)}, bf16[4,1408,256]{2,1,0:T(8,128)(2,1)S(1)}, u32[]{:S(2)}, u32[]{:S(2)}) collective-permute-start(bf16[4,1408,256]{2,1,0:T(8,128)(2,1)} %bitcast.205), channel_id=1, source_target_pairs={{0,16},{16,0},{1,17},{17,1},{2,18},{18,2},{3,19},{19,3},{4,20},{20... | collective-permute-start | bytes 8650760 | tf_op jit(solution)/shard_map/ppermute | solution.py:51
  336.2 4.2 %collective-permute-start.17 = (bf16[2,128,1024]{2,1,0:T(8,128)(2,1)S(1)}, bf16[2,128,1024]{2,1,0:T(8,128)(2,1)S(1)}, u32[]{:S(2)}, u32[]{:S(2)}) collective-permute-start(bf16[2,128,1024]{2,1,0:T(8,128)(2,1)S(1)} %dynamic-slice_bitcast_fusion), channel_id=1, source_target_pairs={{0,1},{1,0},{2,3},{3,2},{4,5},{5,4},{6,7},{7,6},{8,9},{9,8},{10,11... | collective-permute-start | bytes 1572872 | tf_op jit(solution)/shard_map/ppermute | solution.py:55
  340.3 2.0 collective-permute-start.14
  340.6 9.2 %collective-permute-start.18 = (bf16[128,1024]{1,0:T(8,128)(2,1)S(1)}, bf16[128,1024]{1,0:T(8,128)(2,1)S(1)}, u32[]{:S(2)}, u32[]{:S(2)}) collective-permute-start(bf16[128,1024]{1,0:T(8,128)(2,1)S(1)} %fusion.40), channel_id=1, source_target_pairs={{0,2},{1,3},{2,0},{3,1},{4,6},{5,7},{6,4},{7,5},{8,10},{9,11},{10,... | collective-permute-start | bytes 786440 | tf_op jit(solution)/shard_map/ppermute | solution.py:51
  342.5 12.5 %collective-permute-start.15 = (bf16[128,1024]{1,0:T(8,128)(2,1)S(1)}, bf16[128,1024]{1,0:T(8,128)(2,1)S(1)}, u32[]{:S(2)}, u32[]{:S(2)}) collective-permute-start(bf16[128,1024]{1,0:T(8,128)(2,1)S(1)} %fusion.39), channel_id=1, source_target_pairs={{0,2},{1,3},{2,0},{3,1},{4,6},{5,7},{6,4},{7,5},{8,10},{9,11},{10,... | collective-permute-start | bytes 786440 | tf_op jit(solution)/shard_map/ppermute | solution.py:51
  (18 other events, 124.2 us)
Sparse Core Ops, SparseCore 0:
  8.9 48.3 all-gather.7
  58.9 26.7 all-gather.13
  87.3 58.4 all-gather.9
  147.2 57.7 all-gather.11
  206.5 57.7 all-gather.15
where the time goes:
time: 364 us
  waiting for transfers between devices  258 us (71%)
  matrix products  35.6 us (10%)
  local copies, waits for them, and re-layouts  27.2 us (7%)
  starting transfers between devices  17.8 us (5%)
  between operations  14.1 us (4%)
  other arithmetic  10.4 us (3%)
    ppermute x11, waiting for transfers between devices, shift(): lax.ppermute(values, axis, [(i, (i + distance) % count) for i in range(co...  101 us
    all_gather x3, waiting for transfers between devices, row_parts(): own = lax.all_gather(own, 'fs', axis=0, tiled=True)  80.2 us
    all_gather x2, waiting for transfers between devices, column_parts(): own = lax.all_gather(own, 'fs', axis=0, tiled=False)  76.9 us
    ppermute x11, starting transfers between devices, shift(): lax.ppermute(values, axis, [(i, (i + distance) % count) for i in range(co...  17 us
    dot_general x16, matrix products, project_out(): jnp.dot(values, weight[g], preferred_element_type=jnp.float32)  11 us
    dot_general x3, matrix products, dots(): total = total + jnp.dot(left, right, preferred_element_type=jnp.float32)  10.9 us
  transfers between devices with their start and end apart: 24, of which 13 were waited for; matrix products, arithmetic and copies ran while one was open for 17% of the time, Pallas kernels for 0%

commit v1 on v0

--- a/solution.py
+++ b/solution.py
@@ -1,6 +1,8 @@
 import jax
 import jax.numpy as jnp
 from jax import lax
+from jax.experimental import pallas as pl
+from jax.experimental.pallas import tpu as pltpu
 from jax.sharding import PartitionSpec as P
 
 KEY_CHANNELS = 128
@@ -211,9 +213,523 @@
     return hidden + project_out(activated, down_weights)
 
 
+BF16 = jnp.bfloat16
+F32 = jnp.float32
+MESH_ID = pl.DeviceIdType.MESH
+KINDS = ("end_a", "end_b", "mid_own", "mid_end", "rep_own", "rep_end")
+PARTS = ("qkv", "out", "gate0", "up0", "gate1", "up1", "down")
+
+
+def layer_kernel(
+    tokens, mix_gain, w_query, w_key, w_value, w_decay_down, w_decay_up, decay_bias,
+    decay_shift, head_gain, w_mix_out, ffn_gain, w_gate, w_up, w_down,
+    out,
+    wq, wo, wg, wu, wd, tok, shift, x_mix, x_ffn, proj, gated, part, near, far, near2, far2,
+    act, hid, mixed_home, ffn_home, state,
+    load_sem, w_send, w_recv, a_send, a_recv,
+):
+    r, z, t = lax.axis_index("rep"), lax.axis_index("fs"), lax.axis_index("tp")
+    depth, key_cols = w_query.shape
+    value_cols = w_value.shape[1]
+    rows, width = tokens.shape
+    seq = rows * 4
+    hidden_units = w_gate.shape[1]
+    block = width // 8
+    half_rows = depth // 2
+    cut = (hidden_units // 256 + 1) // 2 * 256
+    heads = key_cols // KEY_CHANNELS
+    zc = 1 + z // 2
+    ze = 3 * (z // 2)
+    zo, zf = 3 - zc, 3 - ze
+    other_r = 1 - r
+    core = t + 1 - 2 * lax.rem(t, 2)
+    chip = lax.rem(t + 2, 4)
+    both = 3 - t
+    pair_z = z + 1 - 2 * lax.rem(z, 2)
+    is_centre = jnp.logical_and(z >= 1, z <= 2)
+
+    barrier = pltpu.get_barrier_semaphore()
+    for partner in ({"fs": pair_z}, {"fs": 3 - z}, {"rep": other_r}, {"tp": core}, {"tp": chip}):
+        pl.semaphore_signal(barrier, inc=1, device_id=partner, device_id_type=MESH_ID)
+
+    def region(name, plane, half):
+        at = pl.multiple_of(plane * depth + half * half_rows, half_rows)
+        if name == "qkv":
+            return wq.at[pl.ds(at, half_rows), :]
+        if name == "out":
+            return wo.at[2 * plane + half]
+        if name == "down":
+            return wd.at[2 * plane + half]
+        ref = wg if name.startswith("gate") else wu
+        if name.endswith("0"):
+            return ref.at[pl.ds(at, half_rows), pl.ds(0, cut)]
+        return ref.at[pl.ds(at, half_rows), pl.ds(cut, hidden_units - cut)]
+
+    def weight_copy(name, kind, plane, half, device):
+        ref = region(name, plane, half)
+        index = PARTS.index(name) * len(KINDS) + KINDS.index(kind)
+        return pltpu.make_async_remote_copy(
+            src_ref=ref, dst_ref=ref, send_sem=w_send.at[index], recv_sem=w_recv.at[index],
+            device_id=device, device_id_type=MESH_ID,
+        )
+
+    names = iter(range(1000))
+    act_ids = {}
+
+    def act_copy(key, src, dst, device):
+        index = act_ids.setdefault(key, len(act_ids))
+        return pltpu.make_async_remote_copy(
+            src_ref=src, dst_ref=dst, send_sem=a_send.at[index], recv_sem=a_recv.at[index],
+            device_id=device, device_id_type=MESH_ID,
+        )
+
+    at_z = pl.multiple_of(z * depth, depth)
+    loads = {}
+
+    def load(name, src, dst):
+        copy = pltpu.make_async_copy(src, dst, load_sem.at[len(loads)])
+        copy.start()
+        loads[name] = copy
+
+    load("q", w_query, wq.at[pl.ds(at_z, depth), pl.ds(0, key_cols)])
+    load("k", w_key, wq.at[pl.ds(at_z, depth), pl.ds(key_cols, key_cols)])
+    load("v", w_value, wq.at[pl.ds(at_z, depth), pl.ds(2 * key_cols, value_cols)])
+    load("tok", tokens, tok.at[0])
+    load("o0", w_mix_out.at[:, pl.ds(0, block)], wo.at[2 * z])
+    load("o1", w_mix_out.at[:, pl.ds(block, block)], wo.at[2 * z + 1])
+    load("shift", decay_shift, shift.at[0])
+    load("g", w_gate, wg.at[pl.ds(at_z, depth), :])
+    load("u", w_up, wu.at[pl.ds(at_z, depth), :])
+    load("d0", w_down.at[:, pl.ds(0, block)], wd.at[2 * z])
+    load("d1", w_down.at[:, pl.ds(block, block)], wd.at[2 * z + 1])
+    pl.semaphore_wait(barrier, 5)
+    for name in ("q", "k", "v"):
+        loads[name].wait()
+
+    tok_copy = act_copy("tok", tok.at[0], tok.at[1], {"fs": pair_z})
+    shift_copy = act_copy("shift", shift.at[0], shift.at[1], {"fs": pair_z})
+
+    out_order = [
+        (2 * zc, None), (2 * zc + 1, None),
+        (2 * zo + r, ("mid_own", zo, r)), (2 * ze + r, ("end_a", ze, r)),
+        (2 * zo + other_r, ("rep_own", zo, other_r)), (2 * zf + r, ("mid_end", zf, r)),
+        (2 * ze + other_r, ("end_b", ze, other_r)), (2 * zf + other_r, ("rep_end", zf, other_r)),
+    ]
+    mixed_copy = act_copy("mixed", mixed_home, mixed_home, {"fs": pair_z})
+    home_copies = [
+        act_copy(("home", i), ffn_home.at[b], ffn_home.at[b], {"fs": pair_z})
+        for i, (b, _) in enumerate(out_order)
+    ]
+
+    @pl.when(jnp.logical_not(is_centre))
+    def _():
+        sent = []
+
+        def send(name, kind, half):
+            copy = weight_copy(name, kind, z, half, {"fs": pair_z})
+            copy.start()
+            sent.append(copy)
+
+        send("qkv", "end_a", r)
+        loads["tok"].wait()
+        tok_copy.start()
+        loads["o0"].wait()
+        loads["o1"].wait()
+        send("out", "end_a", r)
+        send("qkv", "end_b", other_r)
+        loads["shift"].wait()
+        shift_copy.start()
+        loads["g"].wait()
+        loads["u"].wait()
+        send("gate0", "end_a", r)
+        send("up0", "end_a", r)
+        send("out", "end_b", other_r)
+        send("gate0", "end_b", other_r)
+        send("up0", "end_b", other_r)
+        send("gate1", "end_a", r)
+        send("up1", "end_a", r)
+        loads["d0"].wait()
+        loads["d1"].wait()
+        send("down", "end_a", r)
+        send("gate1", "end_b", other_r)
+        send("up1", "end_b", other_r)
+        send("down", "end_b", other_r)
+        mixed_copy.wait_recv()
+        for i, (b, _) in enumerate(out_order):
+            home_copies[i].wait_recv()
+            cols = pl.ds(pl.multiple_of(b * block, block), block)
+            out[:, cols] = (
+                tok[0, :, cols].astype(F32) + mixed_home[b].astype(F32) + ffn_home[b].astype(F32)
+            )
+        tok_copy.wait_send()
+        shift_copy.wait_send()
+        for copy in sent:
+            copy.wait_send()
+
+    @pl.when(is_centre)
+    def _():
+        sent = []
+
+        def incoming(name, kind, plane, half):
+            weight_copy(name, kind, plane, half, {"fs": pair_z}).wait_recv()
+
+        def send(name, kind, plane, half, device):
+            copy = weight_copy(name, kind, plane, half, device)
+            copy.start()
+            sent.append(copy)
+
+        def mid_own(*parts):
+            for name in parts:
+                send(name, "mid_own", z, r, {"fs": zo})
+
+        def mid_end(*parts):
+            for name in parts:
+                incoming(name, "end_a", ze, r)
+                send(name, "mid_end", ze, r, {"fs": zo})
+
+        def rep_own(*parts):
+            for name in parts:
+                incoming(name, "mid_own", zo, r)
+                send(name, "rep_own", zo, r, {"rep": other_r})
+
+        def rep_end(*parts):
+            for name in parts:
+                incoming(name, "mid_end", zf, r)
+                send(name, "rep_end", zf, r, {"rep": other_r})
+
+        def complete(*parts):
+            for name in parts:
+                incoming(name, "end_b", ze, other_r)
+                incoming(name, "rep_own", zo, other_r)
+                incoming(name, "rep_end", zf, other_r)
+
+        def norm_rows(load_rows, gain, dst, s):
+            @pl.loop(0, rows // 16)
+            def _(i):
+                values = load_rows(pl.ds(pl.multiple_of(i * 16, 16), 16))
+                scale = lax.rsqrt(jnp.mean(values * values, axis=-1, keepdims=True) + EPS)
+                at = pl.multiple_of(t * rows + i * 16, 16)
+                dst[s, pl.ds(at, 16), :] = (values * scale * gain[...]).astype(BF16)
+
+        class Gather:
+            def __init__(self, key, ref, s):
+                def rows_of(device):
+                    return ref.at[s, pl.ds(pl.multiple_of(device * rows, rows), rows), :]
+
+                mine, theirs = rows_of(t), rows_of(chip)
+                self.to_chip = act_copy((key, s, "chip"), mine, mine, {"tp": chip})
+                self.to_core = act_copy((key, s, "core"), mine, mine, {"tp": core})
+                self.pass_on = act_copy((key, s, "pass"), theirs, theirs, {"tp": core})
+                self.from_chip = act_copy((key, s, "chip"), theirs, theirs, {"tp": chip})
+                self.from_core = act_copy((key, s, "core"), rows_of(core), rows_of(core), {"tp": core})
+                self.passed = act_copy((key, s, "pass"), rows_of(both), rows_of(both), {"tp": core})
+
+            def start(self):
+                self.to_chip.start()
+                self.to_core.start()
+
+            def forward(self):
+                self.from_chip.wait_recv()
+                self.pass_on.start()
+
+            def finish(self):
+                self.from_core.wait_recv()
+                self.passed.wait_recv()
+
+            def drain(self):
+                self.to_chip.wait_send()
+                self.to_core.wait_send()
+                self.pass_on.wait_send()
+
+        mid_own("qkv")
+        loads["o0"].wait()
+        loads["o1"].wait()
+        mid_own("out")
+        loads["tok"].wait()
+        norm_rows(lambda at: tok[0, at, :].astype(F32), mix_gain, x_mix, 0)
+        mix_gather = [Gather("mix", x_mix, s) for s in range(2)]
+        ffn_gather = [Gather("ffn", x_ffn, s) for s in range(2)]
+        mix_gather[0].start()
+        loads["shift"].wait()
+        loads["g"].wait()
+        loads["u"].wait()
+        mid_end("qkv")
+        rep_own("qkv")
+        mix_gather[0].forward()
+        mid_own("gate0", "up0")
+        tok_copy.wait_recv()
+        norm_rows(lambda at: tok[1, at, :].astype(F32), mix_gain, x_mix, 1)
+        mix_gather[1].start()
+        rep_end("qkv")
+        mid_end("out")
+        rep_own("out")
+        mid_own("gate1", "up1")
+        mix_gather[1].forward()
+        loads["d0"].wait()
+        loads["d1"].wait()
+        mix_gather[0].finish()
+        mix_gather[1].finish()
+        complete("qkv")
+
+        bias = decay_bias[:, pl.ds(pl.multiple_of(t * key_cols, key_cols), key_cols)]
+        up_cols = w_decay_up[:, pl.ds(pl.multiple_of(t * key_cols, key_cols), key_cols)]
+
+        def project(s):
+            @pl.loop(0, seq // 256)
+            def _(i):
+                at = pl.ds(pl.multiple_of(i * 256, 256), 256)
+                x = x_mix[s, at, :]
+                for n in range(0, 2 * key_cols + value_cols, 512):
+                    cols = pl.ds(n, 512)
+                    proj[s, at, cols] = jnp.dot(x, wq[:, cols], preferred_element_type=F32).astype(BF16)
+                low = jnp.dot(x, w_decay_down[...], preferred_element_type=F32).astype(BF16)
+                pre = jnp.dot(low, up_cols, preferred_element_type=F32) + bias
+                log_sig = jnp.minimum(pre, 0.0) - jnp.log1p(jnp.exp(-jnp.abs(pre)))
+                shift[s, at, :] = log_sig / TAU + shift[s, at, :]
+
+        lower = (
+            lax.broadcasted_iota(jnp.int32, (BLK, BLK), 0) >= lax.broadcasted_iota(jnp.int32, (BLK, BLK), 1)
+        )
+        gain_cols = head_gain[:, pl.ds(pl.multiple_of(t * value_cols, value_cols), value_cols)]
+
+        def attend(s):
+            state[...] = jnp.zeros_like(state)
+
+            @pl.loop(0, seq // BLK)
+            def _(b):
+                at = pl.ds(pl.multiple_of(b * BLK, BLK), BLK)
+                for h in range(heads):
+                    key_at = pl.ds(h * KEY_CHANNELS, KEY_CHANNELS)
+                    decays = shift[s, at, key_at]
+                    cumul = jnp.dot(
+                        lower.astype(F32), decays, precision=lax.Precision.HIGHEST,
+                        preferred_element_type=F32,
+                    )
+                    total = cumul[BLK - 1 :, :]
+                    queries = proj[s, at, key_at].astype(F32) * KEY_CHANNELS ** (-0.5)
+                    keys = proj[s, at, pl.ds(key_cols + h * KEY_CHANNELS, KEY_CHANNELS)].astype(F32)
+                    values = proj[s, at, pl.ds(2 * key_cols + h * DV, DV)]
+                    q_decayed = (queries * jnp.exp(cumul)).astype(BF16)
+                    k_decayed = (keys * jnp.exp(-cumul)).astype(BF16)
+                    weighted = (keys * jnp.exp(total - cumul)).astype(BF16)
+                    scores = lax.dot_general(
+                        q_decayed, k_decayed, (((1,), (1,)), ((), ())), preferred_element_type=F32
+                    )
+                    scores = jnp.where(lower, scores, 0.0).astype(BF16)
+                    before = state[h]
+                    result = jnp.dot(scores, values, preferred_element_type=F32) + lax.dot_general(
+                        q_decayed, before.astype(BF16), (((1,), (1,)), ((), ())), preferred_element_type=F32
+                    )
+                    state[h] = jnp.exp(total) * before + lax.dot_general(
+                        values, weighted, (((0,), (0,)), ((), ())), preferred_element_type=F32
+                    )
+                    scale = lax.rsqrt(jnp.mean(result * result, axis=-1, keepdims=True) + EPS)
+                    gated[s, at, pl.ds(h * DV, DV)] = (
+                        result * scale * gain_cols[:, h * DV : (h + 1) * DV]
+                    ).astype(BF16)
+
+        def mix_out(s):
+            @pl.loop(0, 8)
+            def _(b):
+                value = jnp.dot(gated[s], wo[b], preferred_element_type=F32).astype(BF16)
+                for k in range(4):
+                    part[b, k, s] = value[k * rows : (k + 1) * rows]
+
+        def reduce_copies(s):
+            return (
+                act_copy(("red", s, 0), part.at[:, core, s], near.at[0, s], {"tp": core}),
+                act_copy(("red", s, 1), part.at[:, both, s], near.at[1, s], {"tp": core}),
+                act_copy(("red", s, 2), part.at[:, chip, s], far.at[s], {"tp": chip}),
+            )
+
+        reduce = [reduce_copies(s) for s in range(2)]
+
+        def reduce_far(s):
+            reduce[s][1].wait_recv()
+
+            @pl.loop(0, 8)
+            def _(b):
+                total = part[b, chip, s].astype(F32) + near[1, s, b].astype(F32)
+                part[b, chip, s] = total.astype(BF16)
+
+            reduce[s][2].start()
+
+        def reduce_end(s):
+            reduce[s][0].wait_recv()
+            reduce[s][2].wait_recv()
+            for b in range(8):
+                cols = pl.ds(b * block, block)
+                total = part[b, t, s].astype(F32) + near[0, s, b].astype(F32) + far[s, b].astype(F32)
+                hid[s, :, cols] = tok[s, :, cols].astype(F32) + total
+                if s == 1:
+                    mixed_home[b] = total.astype(BF16)
+            if s == 1:
+                mixed_copy.start()
+            norm_rows(lambda at: hid[s, at, :], ffn_gain, x_ffn, s)
+            ffn_gather[s].start()
+
+        project(0)
+        rep_end("out")
+        rep_own("gate0", "up0")
+        shift_copy.wait_recv()
+        project(1)
+        attend(0)
+        rep_own("gate1", "up1")
+        complete("out")
+        mix_out(0)
+        reduce[0][1].start()
+        reduce[0][0].start()
+        attend(1)
+        reduce_far(0)
+        mid_end("gate0", "up0")
+        mid_own("down")
+        mix_out(1)
+        reduce[1][1].start()
+        reduce[1][0].start()
+        reduce_end(0)
+        reduce_far(1)
+        ffn_gather[0].forward()
+        reduce_end(1)
+        rep_end("gate0", "up0")
+        ffn_gather[0].finish()
+        ffn_gather[1].forward()
+        complete("gate0", "up0")
+
+        def expand(s, lo, hi):
+            @pl.loop(0, seq // 256)
+            def _(i):
+                at = pl.ds(pl.multiple_of(i * 256, 256), 256)
+                x = x_ffn[s, at, :]
+                for n in range(lo, hi, 256):
+                    cols = pl.ds(n, min(256, hi - n))
+                    gate = jnp.dot(x, wg[:, cols], preferred_element_type=F32)
+                    up = jnp.dot(x, wu[:, cols], preferred_element_type=F32)
+                    act[s, at, cols] = (gate / (1.0 + jnp.exp(-gate)) * up).astype(BF16)
+
+        expand(0, 0, cut)
+        mid_end("gate1", "up1")
+        rep_own("down")
+        ffn_gather[1].finish()
+        expand(1, 0, cut)
+        mid_end("down")
+        rep_end("gate1", "up1")
+        complete("gate1", "up1")
+        expand(0, cut, hidden_units)
+        rep_end("down")
+        expand(1, cut, hidden_units)
+        for s in range(2):
+            for copy in reduce[s]:
+                copy.wait_send()
+
+        def piece_copies(i, b):
+            return (
+                act_copy(("piece", i, 0), part.at[b, core], near2.at[i, 0], {"tp": core}),
+                act_copy(("piece", i, 1), part.at[b, both], near2.at[i, 1], {"tp": core}),
+                act_copy(("piece", i, 2), part.at[b, chip], far2.at[i], {"tp": chip}),
+            )
+
+        pieces = [piece_copies(i, b) for i, (b, _) in enumerate(out_order)]
+        waited = ("mid_own", "end_a", "mid_end")
+        for i in range(len(out_order) + 2):
+            if i < len(out_order):
+                b, source = out_order[i]
+                if source is not None and source[0] not in waited:
+                    incoming("down", *source)
+                for s in range(2):
+                    value = jnp.dot(act[s], wd[b], preferred_element_type=F32).astype(BF16)
+                    for k in range(4):
+                        part[b, k, s] = value[k * rows : (k + 1) * rows]
+                pieces[i][1].start()
+                pieces[i][0].start()
+            if 1 <= i <= len(out_order):
+                b = out_order[i - 1][0]
+                pieces[i - 1][1].wait_recv()
+                part[b, chip] = (part[b, chip].astype(F32) + near2[i - 1, 1].astype(F32)).astype(BF16)
+                pieces[i - 1][2].start()
+            if i >= 2:
+                b = out_order[i - 2][0]
+                pieces[i - 2][0].wait_recv()
+                pieces[i - 2][2].wait_recv()
+                total = part[b, t].astype(F32) + near2[i - 2, 0].astype(F32) + far2[i - 2].astype(F32)
+                cols = pl.ds(pl.multiple_of(b * block, block), block)
+                ffn_home[b] = total[1].astype(BF16)
+                home_copies[i - 2].start()
+                out[:, cols] = hid[0, :, cols] + total[0]
+        for gather in mix_gather + ffn_gather:
+            gather.drain()
+        for copies in pieces:
+            for copy in copies:
+                copy.wait_send()
+        mixed_copy.wait_send()
+        for copy in home_copies:
+            copy.wait_send()
+        for copy in sent:
+            copy.wait_send()
+
+
+def per_device_kernel(
+    tokens, mix_gain, w_query, w_key, w_value, w_decay_down, w_decay_up, decay_bias,
+    decay_shift, head_gain, w_mix_out, ffn_gain, w_gate, w_up, w_down,
+):
+    rows, width = tokens.shape
+    planes, tps = lax.axis_size("fs"), lax.axis_size("tp")
+    key_cols, value_cols, hidden_units = w_query.shape[1], w_value.shape[1], w_gate.shape[1]
+    depth = w_query.shape[0]
+    seq = rows * tps
+    blocks = 2 * planes
+    block = width // blocks
+    any_spec = pl.BlockSpec(memory_space=pl.ANY)
+    vmem_spec = pl.BlockSpec(memory_space=pltpu.VMEM)
+    large = {0, 2, 3, 4, 8, 10, 12, 13, 14}
+    args = (
+        tokens, mix_gain.reshape(1, -1), w_query, w_key, w_value, w_decay_down, w_decay_up,
+        decay_bias.reshape(1, -1), decay_shift, head_gain.reshape(1, -1), w_mix_out,
+        ffn_gain.reshape(1, -1), w_gate, w_up, w_down,
+    )
+    return pl.pallas_call(
+        layer_kernel,
+        out_shape=jax.ShapeDtypeStruct((rows, width), F32),
+        in_specs=[any_spec if i in large else vmem_spec for i in range(len(args))],
+        out_specs=vmem_spec,
+        scratch_shapes=[
+            pltpu.VMEM((planes * depth, 2 * key_cols + value_cols), BF16),
+            pltpu.VMEM((blocks, value_cols, block), BF16),
+            pltpu.VMEM((planes * depth, hidden_units), BF16),
+            pltpu.VMEM((planes * depth, hidden_units), BF16),
+            pltpu.VMEM((blocks, hidden_units, block), BF16),
+            pltpu.VMEM((2, rows, width), BF16),
+            pltpu.VMEM((2, seq, key_cols), F32),
+            pltpu.VMEM((2, seq, width), BF16),
+            pltpu.VMEM((2, seq, width), BF16),
+            pltpu.VMEM((2, seq, 2 * key_cols + value_cols), BF16),
+            pltpu.VMEM((2, seq, value_cols), BF16),
+            pltpu.VMEM((blocks, tps, 2, rows, block), BF16),
+            pltpu.VMEM((2, 2, blocks, rows, block), BF16),
+            pltpu.VMEM((2, blocks, rows, block), BF16),
+            pltpu.VMEM((blocks, 2, 2, rows, block), BF16),
+            pltpu.VMEM((blocks, 2, rows, block), BF16),
+            pltpu.VMEM((2, seq, hidden_units), BF16),
+            pltpu.VMEM((2, rows, width), F32),
+            pltpu.VMEM((blocks, rows, block), BF16),
+            pltpu.VMEM((blocks, rows, block), BF16),
+            pltpu.VMEM((key_cols // KEY_CHANNELS, DV, KEY_CHANNELS), F32),
+            pltpu.SemaphoreType.DMA((16,)),
+            pltpu.SemaphoreType.DMA((len(PARTS) * len(KINDS),)),
+            pltpu.SemaphoreType.DMA((len(PARTS) * len(KINDS),)),
+            pltpu.SemaphoreType.DMA((64,)),
+            pltpu.SemaphoreType.DMA((64,)),
+        ],
+        compiler_params=pltpu.CompilerParams(
+            collective_id=0, has_side_effects=True, vmem_limit_bytes=67043328
+        ),
+    )(*args)
+
+
 def solution(mesh):
+    shape = dict(mesh.shape)
+    small = shape["rep"] == 2 and shape["fs"] == 4 and shape["tp"] == 4
     return jax.shard_map(
-        per_device,
+        per_device_kernel if small else per_device,
         mesh=mesh,
         in_specs=(
             P(("rep", "fs", "tp"), None),

time: 364 us -> 218 us (0.60)
  waiting for transfers between devices: 258 us -> 0 us
  Pallas kernels: 0 us -> 214 us
  matrix products: 35.6 us -> 0 us
  local copies, waits for them, and re-layouts: 27.2 us -> 4.2 us
  starting transfers between devices: 17.8 us -> 0 us
  between operations: 14.1 us -> 0.01 us
  other arithmetic: 10.4 us -> 0 us
    pallas_call x0 -> x1, Pallas kernels: none -> 214 us  [per_device_kernel(): pl.pallas_call(layer_kernel, out_shape=jax.ShapeDtypeStruct((rows, width)...]
    all_gather x5 -> x0, waiting for transfers between devices: 157 us -> none  [the longest x3 80.2 us: row_parts(): own = lax.all_gather(own, 'fs', axis=0, tiled=True)]
    ppermute x19 -> x0, waiting for transfers between devices: 101 us -> none  [the longest x11 101 us: shift(): lax.ppermute(values, axis, [(i, (i + distance) % count) for i in range(co...]
    dot_general x28 -> x0, matrix products: 35.6 us -> none  [the longest x16 11 us: project_out(): jnp.dot(values, weight[g], preferred_element_type=jnp.float32)]
    ppermute x19 -> x0, starting transfers between devices: 17.6 us -> none  [the longest x11 17 us: shift(): lax.ppermute(values, axis, [(i, (i + distance) % count) for i in range(co...]
    dynamic_update_slice x6 -> x0, local copies, waits for them, and re-layouts: 6.11 us -> none  [the longest x4 4.41 us: gather_rows(): lax.dynamic_update_slice_in_dim(whole, theirs, (2 * source + 1 - core) *...]
    dynamic_slice x6 -> x0, local copies, waits for them, and re-layouts: 5.06 us -> none  [the longest x2 1.86 us: row_parts(): lax.dynamic_slice_in_dim(weight, lax.axis_index('rep') * share, share, 0)]
    slice x5 -> x0, local copies, waits for them, and re-layouts: 4.07 us -> none  [the longest x2 3.57 us: input_parts(): values[:, (g * reps + j) * share:(g * reps + j + 1) * share]]
  transfers between devices with their start and end apart: 24 -> 0, of which waited for: 13 -> 0; matrix products, arithmetic and copies ran while one was open for 17% -> 0% of each run, Pallas kernels for 0% -> 0%
where the time goes in v1:
time: 218 us
  Pallas kernels  214 us (98%)
  local copies, waits for them, and re-layouts  4.2 us (2%)
    pallas_call x1, Pallas kernels, per_device_kernel(): pl.pallas_call(layer_kernel, out_shape=jax.ShapeDtypeStruct((rows, width)...  214 us

profile of v1, /device:TPU:0, one launch (start us, length us, event | category | flops | bytes accessed | tf_op | source)
XLA Modules:
  0.0 217.8 jit_solution(9999576433814544035)
XLA Ops:
  0.0 1.9 copy.16.w_decay_down
  1.9 213.5 %shard_map.145 = f32[128,2048]{1,0:T(8,128)} custom-call(bf16[128,2048]{1,0:T(8,128)(2,1)} %tokens.1, f32[1,2048]{1,0:T(1,128)} %bitcast.4, bf16[512,256]{1,0:T(8,128)(2,1)} %w_query.1, bf16[512,256]{1,0:T(8,128)(2,1)} %w_key.1, bf16[512,512]{1,0:T(8,128)(2,1)} %w_value.1, bf16[2048,32]{1,0:T(8,128)(2,1)} %copy.16.w_decay_down, bf16[32,1024]{1,0:T(8,128)(2,1)} %w_decay_up.1, ...), custom_call_target="tpu_custom_call" | custom-call | tf_op jit(solution)/shard_map/pallas_call | solution.py:689
  215.5 2.3 %copy.18 = f32[128,2048]{1,0:T(8,128)} copy(f32[128,2048]{1,0:T(8,128)} %shard_map.145) | data formatting | bytes 2097152

commit v2 on v1

--- a/solution.py
+++ b/solution.py
@@ -217,7 +217,8 @@
 F32 = jnp.float32
 MESH_ID = pl.DeviceIdType.MESH
 KINDS = ("end_a", "end_b", "mid_own", "mid_end", "rep_own", "rep_end")
-PARTS = ("qkv", "out", "gate0", "up0", "gate1", "up1", "down")
+PARTS = ("qkv0", "qkv1", "out", "gate0", "up0", "gate1", "up1", "down0", "down1")
+VIA_REP = ("out",)
 
 
 def layer_kernel(
@@ -254,12 +255,14 @@
 
     def region(name, plane, half):
         at = pl.multiple_of(plane * depth + half * half_rows, half_rows)
-        if name == "qkv":
-            return wq.at[pl.ds(at, half_rows), :]
+        if name.startswith("qkv"):
+            piece = half_rows // 2
+            return wq.at[pl.ds(pl.multiple_of(at + int(name[-1]) * piece, piece), piece), :]
         if name == "out":
             return wo.at[2 * plane + half]
-        if name == "down":
-            return wd.at[2 * plane + half]
+        if name.startswith("down"):
+            piece = hidden_units // 2
+            return wd.at[2 * plane + half, pl.ds(int(name[-1]) * piece, piece)]
         ref = wg if name.startswith("gate") else wu
         if name.endswith("0"):
             return ref.at[pl.ds(at, half_rows), pl.ds(0, cut)]
@@ -273,7 +276,6 @@
             device_id=device, device_id_type=MESH_ID,
         )
 
-    names = iter(range(1000))
     act_ids = {}
 
     def act_copy(key, src, dst, device):
@@ -311,9 +313,9 @@
 
     out_order = [
         (2 * zc, None), (2 * zc + 1, None),
-        (2 * zo + r, ("mid_own", zo, r)), (2 * ze + r, ("end_a", ze, r)),
-        (2 * zo + other_r, ("rep_own", zo, other_r)), (2 * zf + r, ("mid_end", zf, r)),
-        (2 * ze + other_r, ("end_b", ze, other_r)), (2 * zf + other_r, ("rep_end", zf, other_r)),
+        (2 * zo + r, None), (2 * ze + r, None), (2 * zo + other_r, ("rep_own", zo, other_r)),
+        (2 * zf + r, None), (2 * ze + other_r, ("end_b", ze, other_r)),
+        (2 * zf + other_r, ("rep_end", zf, other_r)),
     ]
     mixed_copy = act_copy("mixed", mixed_home, mixed_home, {"fs": pair_z})
     home_copies = [
@@ -330,30 +332,33 @@
             copy.start()
             sent.append(copy)
 
-        send("qkv", "end_a", r)
-        loads["tok"].wait()
-        tok_copy.start()
+        send("qkv0", "end_a", r)
+        send("qkv1", "end_a", r)
         loads["o0"].wait()
         loads["o1"].wait()
         send("out", "end_a", r)
-        send("qkv", "end_b", other_r)
+        loads["tok"].wait()
+        tok_copy.start()
+        send("qkv0", "end_b", other_r)
+        send("qkv1", "end_b", other_r)
         loads["shift"].wait()
         shift_copy.start()
         loads["g"].wait()
         loads["u"].wait()
         send("gate0", "end_a", r)
         send("up0", "end_a", r)
-        send("out", "end_b", other_r)
+        send("gate1", "end_a", r)
+        send("up1", "end_a", r)
         send("gate0", "end_b", other_r)
         send("up0", "end_b", other_r)
-        send("gate1", "end_a", r)
-        send("up1", "end_a", r)
+        send("gate1", "end_b", other_r)
+        send("up1", "end_b", other_r)
         loads["d0"].wait()
         loads["d1"].wait()
-        send("down", "end_a", r)
-        send("gate1", "end_b", other_r)
-        send("up1", "end_b", other_r)
-        send("down", "end_b", other_r)
+        send("down0", "end_a", r)
+        send("down1", "end_a", r)
+        send("down0", "end_b", other_r)
+        send("down1", "end_b", other_r)
         mixed_copy.wait_recv()
         for i, (b, _) in enumerate(out_order):
             home_copies[i].wait_recv()
@@ -397,6 +402,10 @@
                 incoming(name, "mid_end", zf, r)
                 send(name, "rep_end", zf, r, {"rep": other_r})
 
+        def rep_end_b(*parts):
+            for name in parts:
+                send(name, "end_b", ze, r, {"rep": other_r})
+
         def complete(*parts):
             for name in parts:
                 incoming(name, "end_b", ze, other_r)
@@ -441,36 +450,14 @@
                 self.to_core.wait_send()
                 self.pass_on.wait_send()
 
-        mid_own("qkv")
-        loads["o0"].wait()
-        loads["o1"].wait()
-        mid_own("out")
+        mid_own("qkv0", "qkv1")
         loads["tok"].wait()
         norm_rows(lambda at: tok[0, at, :].astype(F32), mix_gain, x_mix, 0)
         mix_gather = [Gather("mix", x_mix, s) for s in range(2)]
         ffn_gather = [Gather("ffn", x_ffn, s) for s in range(2)]
         mix_gather[0].start()
-        loads["shift"].wait()
-        loads["g"].wait()
-        loads["u"].wait()
-        mid_end("qkv")
-        rep_own("qkv")
-        mix_gather[0].forward()
-        mid_own("gate0", "up0")
-        tok_copy.wait_recv()
-        norm_rows(lambda at: tok[1, at, :].astype(F32), mix_gain, x_mix, 1)
-        mix_gather[1].start()
-        rep_end("qkv")
-        mid_end("out")
-        rep_own("out")
-        mid_own("gate1", "up1")
-        mix_gather[1].forward()
-        loads["d0"].wait()
-        loads["d1"].wait()
-        mix_gather[0].finish()
-        mix_gather[1].finish()
-        complete("qkv")
-
+        for name in ("o0", "o1", "shift", "g", "u", "d0", "d1"):
+            loads[name].wait()
         bias = decay_bias[:, pl.ds(pl.multiple_of(t * key_cols, key_cols), key_cols)]
         up_cols = w_decay_up[:, pl.ds(pl.multiple_of(t * key_cols, key_cols), key_cols)]
 
@@ -482,7 +469,9 @@
                 for n in range(0, 2 * key_cols + value_cols, 512):
                     cols = pl.ds(n, 512)
                     proj[s, at, cols] = jnp.dot(x, wq[:, cols], preferred_element_type=F32).astype(BF16)
-                low = jnp.dot(x, w_decay_down[...], preferred_element_type=F32).astype(BF16)
+                low = lax.dot_general(
+                    x, w_decay_down[...], (((1,), (1,)), ((), ())), preferred_element_type=F32
+                ).astype(BF16)
                 pre = jnp.dot(low, up_cols, preferred_element_type=F32) + bias
                 log_sig = jnp.minimum(pre, 0.0) - jnp.log1p(jnp.exp(-jnp.abs(pre)))
                 shift[s, at, :] = log_sig / TAU + shift[s, at, :]
@@ -568,33 +557,6 @@
             norm_rows(lambda at: hid[s, at, :], ffn_gain, x_ffn, s)
             ffn_gather[s].start()
 
-        project(0)
-        rep_end("out")
-        rep_own("gate0", "up0")
-        shift_copy.wait_recv()
-        project(1)
-        attend(0)
-        rep_own("gate1", "up1")
-        complete("out")
-        mix_out(0)
-        reduce[0][1].start()
-        reduce[0][0].start()
-        attend(1)
-        reduce_far(0)
-        mid_end("gate0", "up0")
-        mid_own("down")
-        mix_out(1)
-        reduce[1][1].start()
-        reduce[1][0].start()
-        reduce_end(0)
-        reduce_far(1)
-        ffn_gather[0].forward()
-        reduce_end(1)
-        rep_end("gate0", "up0")
-        ffn_gather[0].finish()
-        ffn_gather[1].forward()
-        complete("gate0", "up0")
-
         def expand(s, lo, hi):
             @pl.loop(0, seq // 256)
             def _(i):
@@ -606,21 +568,6 @@
                     up = jnp.dot(x, wu[:, cols], preferred_element_type=F32)
                     act[s, at, cols] = (gate / (1.0 + jnp.exp(-gate)) * up).astype(BF16)
 
-        expand(0, 0, cut)
-        mid_end("gate1", "up1")
-        rep_own("down")
-        ffn_gather[1].finish()
-        expand(1, 0, cut)
-        mid_end("down")
-        rep_end("gate1", "up1")
-        complete("gate1", "up1")
-        expand(0, cut, hidden_units)
-        rep_end("down")
-        expand(1, cut, hidden_units)
-        for s in range(2):
-            for copy in reduce[s]:
-                copy.wait_send()
-
         def piece_copies(i, b):
             return (
                 act_copy(("piece", i, 0), part.at[b, core], near2.at[i, 0], {"tp": core}),
@@ -629,32 +576,132 @@
             )
 
         pieces = [piece_copies(i, b) for i, (b, _) in enumerate(out_order)]
-        waited = ("mid_own", "end_a", "mid_end")
-        for i in range(len(out_order) + 2):
-            if i < len(out_order):
-                b, source = out_order[i]
-                if source is not None and source[0] not in waited:
-                    incoming("down", *source)
-                for s in range(2):
-                    value = jnp.dot(act[s], wd[b], preferred_element_type=F32).astype(BF16)
-                    for k in range(4):
-                        part[b, k, s] = value[k * rows : (k + 1) * rows]
-                pieces[i][1].start()
-                pieces[i][0].start()
-            if 1 <= i <= len(out_order):
-                b = out_order[i - 1][0]
-                pieces[i - 1][1].wait_recv()
-                part[b, chip] = (part[b, chip].astype(F32) + near2[i - 1, 1].astype(F32)).astype(BF16)
-                pieces[i - 1][2].start()
-            if i >= 2:
-                b = out_order[i - 2][0]
-                pieces[i - 2][0].wait_recv()
-                pieces[i - 2][2].wait_recv()
-                total = part[b, t].astype(F32) + near2[i - 2, 0].astype(F32) + far2[i - 2].astype(F32)
-                cols = pl.ds(pl.multiple_of(b * block, block), block)
-                ffn_home[b] = total[1].astype(BF16)
-                home_copies[i - 2].start()
-                out[:, cols] = hid[0, :, cols] + total[0]
+
+        def reduce_start(s):
+            reduce[s][1].start()
+            reduce[s][0].start()
+
+        def reduce_drain():
+            for s in range(2):
+                for copy in reduce[s]:
+                    copy.wait_send()
+
+        def piece_dot(i):
+            b, source = out_order[i]
+            if source is not None:
+                incoming("down0", *source)
+                incoming("down1", *source)
+            for s in range(2):
+                value = jnp.dot(act[s], wd[b], preferred_element_type=F32).astype(BF16)
+                for k in range(4):
+                    part[b, k, s] = value[k * rows : (k + 1) * rows]
+            pieces[i][1].start()
+            pieces[i][0].start()
+
+        def piece_far(i):
+            b = out_order[i][0]
+            pieces[i][1].wait_recv()
+            part[b, chip] = (part[b, chip].astype(F32) + near2[i, 1].astype(F32)).astype(BF16)
+            pieces[i][2].start()
+
+        def piece_end(i):
+            b = out_order[i][0]
+            pieces[i][0].wait_recv()
+            pieces[i][2].wait_recv()
+            total = part[b, t].astype(F32) + near2[i, 0].astype(F32) + far2[i].astype(F32)
+            cols = pl.ds(pl.multiple_of(b * block, block), block)
+            ffn_home[b] = total[1].astype(BF16)
+            home_copies[i].start()
+            out[:, cols] = hid[0, :, cols] + total[0]
+
+        mid_end("qkv0")
+        rep_own("qkv0")
+        mid_end("qkv1")
+        rep_own("qkv1")
+        mix_gather[0].forward()
+        mid_own("out")
+        mid_end("out")
+        mid_own("gate0", "up0")
+        rep_end("qkv0")
+        rep_end("qkv1")
+        tok_copy.wait_recv()
+        norm_rows(lambda at: tok[1, at, :].astype(F32), mix_gain, x_mix, 1)
+        mix_gather[1].start()
+        rep_own("out")
+        rep_end_b("out")
+        rep_end("out")
+        mid_own("gate1", "up1")
+        mix_gather[0].finish()
+        complete("qkv0", "qkv1")
+        project(0)
+        mix_gather[1].forward()
+        rep_own("gate0")
+        attend(0)
+        complete("out")
+        mix_out(0)
+        reduce_start(0)
+        mix_gather[1].finish()
+        shift_copy.wait_recv()
+        project(1)
+        reduce_far(0)
+        rep_own("up0")
+        attend(1)
+        mix_out(1)
+        reduce_start(1)
+        rep_own("gate1")
+        mid_end("gate0")
+        reduce_far(1)
+        rep_own("up1")
+        reduce_end(0)
+        mid_end("up0")
+        rep_end("gate0")
+        reduce_end(1)
+        mid_end("gate1", "up1")
+        mid_own("down0", "down1")
+        rep_end("up0")
+        ffn_gather[0].forward()
+        rep_end("gate1")
+        ffn_gather[0].finish()
+        ffn_gather[1].forward()
+        rep_end("up1")
+        complete("gate0", "up0")
+        expand(0, 0, cut)
+        ffn_gather[1].finish()
+        expand(1, 0, cut)
+        rep_own("down0")
+        rep_own("down1")
+        complete("gate1", "up1")
+        expand(0, cut, hidden_units)
+        expand(1, cut, hidden_units)
+        reduce_drain()
+        mid_end("down0")
+        piece_dot(0)
+        piece_dot(1)
+        piece_far(0)
+        piece_dot(2)
+        piece_far(1)
+        piece_end(0)
+        piece_far(2)
+        piece_end(1)
+        mid_end("down1")
+        rep_end("down0")
+        piece_dot(3)
+        piece_dot(4)
+        piece_far(3)
+        piece_end(2)
+        rep_end("down1")
+        piece_dot(5)
+        piece_far(4)
+        piece_end(3)
+        piece_dot(6)
+        piece_far(5)
+        piece_end(4)
+        piece_dot(7)
+        piece_far(6)
+        piece_end(5)
+        piece_far(7)
+        piece_end(6)
+        piece_end(7)
         for gather in mix_gather + ffn_gather:
             gather.drain()
         for copies in pieces:
@@ -682,7 +729,7 @@
     vmem_spec = pl.BlockSpec(memory_space=pltpu.VMEM)
     large = {0, 2, 3, 4, 8, 10, 12, 13, 14}
     args = (
-        tokens, mix_gain.reshape(1, -1), w_query, w_key, w_value, w_decay_down, w_decay_up,
+        tokens, mix_gain.reshape(1, -1), w_query, w_key, w_value, w_decay_down.T, w_decay_up,
         decay_bias.reshape(1, -1), decay_shift, head_gain.reshape(1, -1), w_mix_out,
         ffn_gain.reshape(1, -1), w_gate, w_up, w_down,
     )

time: 218 us -> 173 us (0.79)
  Pallas kernels: 214 us -> 171 us
    pallas_call x1, Pallas kernels: 214 us -> 171 us  [per_device_kernel(): pl.pallas_call(layer_kernel, out_shape=jax.ShapeDtypeStruct((rows, width)...]
where the time goes in v2:
time: 173 us
  Pallas kernels  171 us (99%)
  local copies, waits for them, and re-layouts  2.3 us (1%)
    pallas_call x1, Pallas kernels, per_device_kernel(): pl.pallas_call(layer_kernel, out_shape=jax.ShapeDtypeStruct((rows, width)...  171 us

profile of v2, /device:TPU:0, one launch (start us, length us, event | category | flops | bytes accessed | tf_op | source)
XLA Modules:
  0.0 173.2 jit_solution(3574243071411045202)
XLA Ops:
  0.0 170.9 %shard_map.145 = f32[128,2048]{1,0:T(8,128)} custom-call(bf16[128,2048]{1,0:T(8,128)(2,1)} %tokens.1, f32[1,2048]{1,0:T(1,128)} %bitcast.6, bf16[512,256]{1,0:T(8,128)(2,1)} %w_query.1, bf16[512,256]{1,0:T(8,128)(2,1)} %w_key.1, bf16[512,512]{1,0:T(8,128)(2,1)} %w_value.1, bf16[32,2048]{1,0:T(8,128)(2,1)} %bitcast.5, bf16[32,1024]{1,0:T(8,128)(2,1)} %w_decay_up.1, ...), custom_call_target="tpu_custom_call" | custom-call | tf_op jit(solution)/shard_map/pallas_call | solution.py:736
  170.9 2.3 %copy.17 = f32[128,2048]{1,0:T(8,128)} copy(f32[128,2048]{1,0:T(8,128)} %shard_map.145) | data formatting | bytes 2097152

commit v3 on v2

--- a/solution.py
+++ b/solution.py
@@ -217,8 +217,8 @@
 F32 = jnp.float32
 MESH_ID = pl.DeviceIdType.MESH
 KINDS = ("end_a", "end_b", "mid_own", "mid_end", "rep_own", "rep_end")
-PARTS = ("qkv0", "qkv1", "out", "gate0", "up0", "gate1", "up1", "down0", "down1")
-VIA_REP = ("out",)
+PARTS = ("qkv0", "qkv1", "out", "gate0", "up0", "gate1", "up1", "down0", "down1", "down2", "down3")
+DOWN = PARTS[-4:]
 
 
 def layer_kernel(
@@ -226,7 +226,7 @@
     decay_shift, head_gain, w_mix_out, ffn_gain, w_gate, w_up, w_down,
     out,
     wq, wo, wg, wu, wd, tok, shift, x_mix, x_ffn, proj, gated, part, near, far, near2, far2,
-    act, hid, mixed_home, ffn_home, state,
+    act, hid, mixed_home, ffn_home, state, shift_sent,
     load_sem, w_send, w_recv, a_send, a_recv,
 ):
     r, z, t = lax.axis_index("rep"), lax.axis_index("fs"), lax.axis_index("tp")
@@ -261,7 +261,7 @@
         if name == "out":
             return wo.at[2 * plane + half]
         if name.startswith("down"):
-            piece = hidden_units // 2
+            piece = hidden_units // 4
             return wd.at[2 * plane + half, pl.ds(int(name[-1]) * piece, piece)]
         ref = wg if name.startswith("gate") else wu
         if name.endswith("0"):
@@ -309,13 +309,13 @@
         loads[name].wait()
 
     tok_copy = act_copy("tok", tok.at[0], tok.at[1], {"fs": pair_z})
-    shift_copy = act_copy("shift", shift.at[0], shift.at[1], {"fs": pair_z})
+    shift_copy = act_copy("shift", shift_sent.at[0], shift_sent.at[1], {"fs": pair_z})
 
     out_order = [
         (2 * zc, None), (2 * zc + 1, None),
-        (2 * zo + r, None), (2 * ze + r, None), (2 * zo + other_r, ("rep_own", zo, other_r)),
-        (2 * zf + r, None), (2 * ze + other_r, ("end_b", ze, other_r)),
-        (2 * zf + other_r, ("rep_end", zf, other_r)),
+        (2 * zo + r, ("mid_own", zo, r)), (2 * ze + r, ("end_a", ze, r)),
+        (2 * zo + other_r, ("rep_own", zo, other_r)), (2 * zf + r, ("mid_end", zf, r)),
+        (2 * ze + other_r, ("end_b", ze, other_r)), (2 * zf + other_r, ("rep_end", zf, other_r)),
     ]
     mixed_copy = act_copy("mixed", mixed_home, mixed_home, {"fs": pair_z})
     home_copies = [
@@ -340,32 +340,25 @@
         loads["tok"].wait()
         tok_copy.start()
         send("qkv0", "end_b", other_r)
-        send("qkv1", "end_b", other_r)
         loads["shift"].wait()
+        shift_sent[0] = shift[0].astype(BF16)
         shift_copy.start()
-        loads["g"].wait()
-        loads["u"].wait()
-        send("gate0", "end_a", r)
-        send("up0", "end_a", r)
-        send("gate1", "end_a", r)
-        send("up1", "end_a", r)
-        send("gate0", "end_b", other_r)
-        send("up0", "end_b", other_r)
-        send("gate1", "end_b", other_r)
-        send("up1", "end_b", other_r)
-        loads["d0"].wait()
-        loads["d1"].wait()
-        send("down0", "end_a", r)
-        send("down1", "end_a", r)
-        send("down0", "end_b", other_r)
-        send("down1", "end_b", other_r)
+        send("out", "end_b", other_r)
+        for name in ("g", "u", "d0", "d1"):
+            loads[name].wait()
+        for name in ("gate0", "up0", "gate1", "up1"):
+            send(name, "end_a", r)
+        for name in ("gate0", "up0", "gate1", "up1"):
+            send(name, "end_b", other_r)
+        for name in DOWN:
+            send(name, "end_a", r)
+        for name in DOWN:
+            send(name, "end_b", other_r)
         mixed_copy.wait_recv()
         for i, (b, _) in enumerate(out_order):
             home_copies[i].wait_recv()
             cols = pl.ds(pl.multiple_of(b * block, block), block)
-            out[:, cols] = (
-                tok[0, :, cols].astype(F32) + mixed_home[b].astype(F32) + ffn_home[b].astype(F32)
-            )
+            out[:, cols] = mixed_home[b].astype(F32) + ffn_home[b].astype(F32)
         tok_copy.wait_send()
         shift_copy.wait_send()
         for copy in sent:
@@ -375,8 +368,12 @@
     def _():
         sent = []
 
+        arrived = set()
+
         def incoming(name, kind, plane, half):
-            weight_copy(name, kind, plane, half, {"fs": pair_z}).wait_recv()
+            if (name, kind) not in arrived:
+                arrived.add((name, kind))
+                weight_copy(name, kind, plane, half, {"fs": pair_z}).wait_recv()
 
         def send(name, kind, plane, half, device):
             copy = weight_copy(name, kind, plane, half, device)
@@ -404,10 +401,16 @@
 
         def rep_end_b(*parts):
             for name in parts:
+                incoming(name, "end_a", ze, r)
                 send(name, "end_b", ze, r, {"rep": other_r})
+
+        def mid_own_b(*parts):
+            for name in parts:
+                send(name, "rep_own", z, other_r, {"fs": zo})
 
         def complete(*parts):
             for name in parts:
+                incoming(name, "mid_own", zo, r)
                 incoming(name, "end_b", ze, other_r)
                 incoming(name, "rep_own", zo, other_r)
                 incoming(name, "rep_end", zf, other_r)
@@ -474,17 +477,19 @@
                 ).astype(BF16)
                 pre = jnp.dot(low, up_cols, preferred_element_type=F32) + bias
                 log_sig = jnp.minimum(pre, 0.0) - jnp.log1p(jnp.exp(-jnp.abs(pre)))
-                shift[s, at, :] = log_sig / TAU + shift[s, at, :]
+                given = shift[0, at, :] if s == 0 else shift_sent[1, at, :].astype(F32)
+                shift[s, at, :] = log_sig / TAU + given
 
         lower = (
             lax.broadcasted_iota(jnp.int32, (BLK, BLK), 0) >= lax.broadcasted_iota(jnp.int32, (BLK, BLK), 1)
         )
         gain_cols = head_gain[:, pl.ds(pl.multiple_of(t * value_cols, value_cols), value_cols)]
 
-        def attend(s):
-            state[...] = jnp.zeros_like(state)
-
-            @pl.loop(0, seq // BLK)
+        def attend(s, lo, hi):
+            if lo == 0:
+                state[...] = jnp.zeros_like(state)
+
+            @pl.loop(lo, hi)
             def _(b):
                 at = pl.ds(pl.multiple_of(b * BLK, BLK), BLK)
                 for h in range(heads):
@@ -552,6 +557,8 @@
                 hid[s, :, cols] = tok[s, :, cols].astype(F32) + total
                 if s == 1:
                     mixed_home[b] = total.astype(BF16)
+                else:
+                    out[:, cols] = total
             if s == 1:
                 mixed_copy.start()
             norm_rows(lambda at: hid[s, at, :], ffn_gain, x_ffn, s)
@@ -589,8 +596,8 @@
         def piece_dot(i):
             b, source = out_order[i]
             if source is not None:
-                incoming("down0", *source)
-                incoming("down1", *source)
+                for name in DOWN:
+                    incoming(name, *source)
             for s in range(2):
                 value = jnp.dot(act[s], wd[b], preferred_element_type=F32).astype(BF16)
                 for k in range(4):
@@ -612,31 +619,33 @@
             cols = pl.ds(pl.multiple_of(b * block, block), block)
             ffn_home[b] = total[1].astype(BF16)
             home_copies[i].start()
-            out[:, cols] = hid[0, :, cols] + total[0]
-
+            out[:, cols] = out[:, cols] + total[0]
+
+        n_blk = seq // BLK
         mid_end("qkv0")
         rep_own("qkv0")
         mid_end("qkv1")
         rep_own("qkv1")
+        rep_end_b("qkv1")
+        mid_own("out")
         mix_gather[0].forward()
-        mid_own("out")
         mid_end("out")
         mid_own("gate0", "up0")
         rep_end("qkv0")
         rep_end("qkv1")
+        rep_own("out")
+        mix_gather[0].finish()
         tok_copy.wait_recv()
         norm_rows(lambda at: tok[1, at, :].astype(F32), mix_gain, x_mix, 1)
         mix_gather[1].start()
-        rep_own("out")
-        rep_end_b("out")
         rep_end("out")
-        mid_own("gate1", "up1")
-        mix_gather[0].finish()
+        mid_own("gate1")
         complete("qkv0", "qkv1")
         project(0)
+        attend(0, 0, n_blk // 2)
+        rep_own("gate0")
         mix_gather[1].forward()
-        rep_own("gate0")
-        attend(0)
+        attend(0, n_blk // 2, n_blk)
         complete("out")
         mix_out(0)
         reduce_start(0)
@@ -645,60 +654,69 @@
         project(1)
         reduce_far(0)
         rep_own("up0")
-        attend(1)
+        attend(1, 0, n_blk // 2)
+        mid_end("gate0")
+        rep_own("gate1")
+        attend(1, n_blk // 2, n_blk)
         mix_out(1)
         reduce_start(1)
-        rep_own("gate1")
-        mid_end("gate0")
+        mid_end("up0")
+        mid_own("up1")
         reduce_far(1)
+        rep_end("gate0")
+        reduce_end(0)
+        mid_end("gate1")
+        rep_end("up0")
+        mid_end("up1")
+        reduce_end(1)
+        mid_own(*DOWN)
         rep_own("up1")
-        reduce_end(0)
-        mid_end("up0")
-        rep_end("gate0")
-        reduce_end(1)
-        mid_end("gate1", "up1")
-        mid_own("down0", "down1")
-        rep_end("up0")
         ffn_gather[0].forward()
         rep_end("gate1")
+        complete("gate0", "up0")
         ffn_gather[0].finish()
+        rep_end("up1")
+        expand(0, 0, cut)
         ffn_gather[1].forward()
-        rep_end("up1")
-        complete("gate0", "up0")
-        expand(0, 0, cut)
+        rep_own("down0")
         ffn_gather[1].finish()
         expand(1, 0, cut)
-        rep_own("down0")
         rep_own("down1")
         complete("gate1", "up1")
+        rep_own("down2")
         expand(0, cut, hidden_units)
+        rep_own("down3")
+        mid_end("down0")
         expand(1, cut, hidden_units)
+        mid_end("down1")
         reduce_drain()
-        mid_end("down0")
         piece_dot(0)
         piece_dot(1)
         piece_far(0)
+        mid_end("down2")
+        rep_end("down0")
         piece_dot(2)
         piece_far(1)
+        mid_end("down3")
+        piece_dot(3)
+        piece_far(2)
         piece_end(0)
-        piece_far(2)
-        piece_end(1)
-        mid_end("down1")
-        rep_end("down0")
-        piece_dot(3)
+        rep_end("down1")
         piece_dot(4)
         piece_far(3)
+        piece_end(1)
+        rep_end("down2")
+        piece_far(4)
         piece_end(2)
-        rep_end("down1")
+        rep_end("down3")
         piece_dot(5)
-        piece_far(4)
         piece_end(3)
-        piece_dot(6)
         piece_far(5)
         piece_end(4)
-        piece_dot(7)
+        piece_dot(6)
         piece_far(6)
         piece_end(5)
+        piece_dot(7)
         piece_far(7)
         piece_end(6)
         piece_end(7)
@@ -733,7 +751,7 @@
         decay_bias.reshape(1, -1), decay_shift, head_gain.reshape(1, -1), w_mix_out,
         ffn_gain.reshape(1, -1), w_gate, w_up, w_down,
     )
-    return pl.pallas_call(
+    delta = pl.pallas_call(
         layer_kernel,
         out_shape=jax.ShapeDtypeStruct((rows, width), F32),
         in_specs=[any_spec if i in large else vmem_spec for i in range(len(args))],
@@ -760,6 +778,7 @@
             pltpu.VMEM((blocks, rows, block), BF16),
             pltpu.VMEM((blocks, rows, block), BF16),
             pltpu.VMEM((key_cols // KEY_CHANNELS, DV, KEY_CHANNELS), F32),
+            pltpu.VMEM((2, seq, key_cols), BF16),
             pltpu.SemaphoreType.DMA((16,)),
             pltpu.SemaphoreType.DMA((len(PARTS) * len(KINDS),)),
             pltpu.SemaphoreType.DMA((len(PARTS) * len(KINDS),)),
@@ -770,6 +789,7 @@
             collective_id=0, has_side_effects=True, vmem_limit_bytes=67043328
         ),
     )(*args)
+    return tokens.astype(F32) + delta
 
 
 def solution(mesh):

time: 173 us -> 164 us (0.948)
  Pallas kernels: 171 us -> 162 us
  other arithmetic: 0 us -> 2.44 us
  local copies, waits for them, and re-layouts: 2.3 us -> 0 us
    pallas_call x1, Pallas kernels: 171 us -> 162 us  [per_device_kernel(): pl.pallas_call(layer_kernel, out_shape=jax.ShapeDtypeStruct((rows, width)...]
    add x0 -> x1, other arithmetic: none -> 2.44 us  [per_device_kernel(): return tokens.astype(F32) + delta]
    unnamed x1 -> x0, local copies, waits for them, and re-layouts: 2.3 us -> none
where the time goes in v3:
time: 164 us
  Pallas kernels  162 us (99%)
  other arithmetic  2.44 us (1%)
    pallas_call x1, Pallas kernels, per_device_kernel(): pl.pallas_call(layer_kernel, out_shape=jax.ShapeDtypeStruct((rows, width)...  162 us

profile of v3, /device:TPU:0, one launch (start us, length us, event | category | flops | bytes accessed | tf_op | source)
XLA Modules:
  0.0 164.0 jit_solution(2137135353775141615)
XLA Ops:
  0.0 161.5 %shard_map.145 = f32[128,2048]{1,0:T(8,128)} custom-call(bf16[128,2048]{1,0:T(8,128)(2,1)} %tokens.1, f32[1,2048]{1,0:T(1,128)} %bitcast.6, bf16[512,256]{1,0:T(8,128)(2,1)} %w_query.1, bf16[512,256]{1,0:T(8,128)(2,1)} %w_key.1, bf16[512,512]{1,0:T(8,128)(2,1)} %w_value.1, bf16[32,2048]{1,0:T(8,128)(2,1)} %bitcast.5, bf16[32,1024]{1,0:T(8,128)(2,1)} %w_decay_up.1, ...), custom_call_target="tpu_custom_call" | custom-call | tf_op jit(solution)/shard_map/pallas_call | solution.py:754
  161.6 2.4 %convert_add_fusion = f32[128,2048]{1,0:T(8,128)} fusion(f32[128,2048]{1,0:T(8,128)} %shard_map.145, bf16[128,2048]{1,0:T(8,128)(2,1)} %tokens.1), kind=kLoop, calls=%fused_computation | loop fusion | flops 524288 | bytes 2621440 | tf_op jit(solution)/shard_map/add | solution.py:792

commit v4 on v3

--- a/solution.py
+++ b/solution.py
@@ -1,3 +1,5 @@
+import math
+
 import jax
 import jax.numpy as jnp
 from jax import lax
@@ -217,8 +219,10 @@
 F32 = jnp.float32
 MESH_ID = pl.DeviceIdType.MESH
 KINDS = ("end_a", "end_b", "mid_own", "mid_end", "rep_own", "rep_end")
-PARTS = ("qkv0", "qkv1", "out", "gate0", "up0", "gate1", "up1", "down0", "down1", "down2", "down3")
+PARTS = ("qkv0", "qkv1", "qkv2", "qkv3", "out", "gate0", "up0", "gate1", "up1", "down0", "down1", "down2", "down3")
 DOWN = PARTS[-4:]
+GROUPS = {"mix": 0, "ffn": 1, "piece": 2, "home": 2, "mixed": 2, "red": 3, "tok": 4, "shift": 5}
+QKV = PARTS[:4]
 
 
 def layer_kernel(
@@ -226,7 +230,7 @@
     decay_shift, head_gain, w_mix_out, ffn_gain, w_gate, w_up, w_down,
     out,
     wq, wo, wg, wu, wd, tok, shift, x_mix, x_ffn, proj, gated, part, near, far, near2, far2,
-    act, hid, mixed_home, ffn_home, state, shift_sent,
+    act, hid, mixed_home, ffn_home, state, shift_sent, early,
     load_sem, w_send, w_recv, a_send, a_recv,
 ):
     r, z, t = lax.axis_index("rep"), lax.axis_index("fs"), lax.axis_index("tp")
@@ -238,6 +242,8 @@
     block = width // 8
     half_rows = depth // 2
     cut = (hidden_units // 256 + 1) // 2 * 256
+    down_rows = (hidden_units // 2 + 127) // 128 * 128
+    lane = block // 2
     heads = key_cols // KEY_CHANNELS
     zc = 1 + z // 2
     ze = 3 * (z // 2)
@@ -250,19 +256,25 @@
     is_centre = jnp.logical_and(z >= 1, z <= 2)
 
     barrier = pltpu.get_barrier_semaphore()
-    for partner in ({"fs": pair_z}, {"fs": 3 - z}, {"rep": other_r}, {"tp": core}, {"tp": chip}):
+    for partner in (
+        {"fs": pair_z}, {"fs": 3 - z}, {"rep": other_r}, {"tp": core}, {"tp": chip},
+        {"fs": pair_z, "tp": chip},
+    ):
         pl.semaphore_signal(barrier, inc=1, device_id=partner, device_id_type=MESH_ID)
 
     def region(name, plane, half):
         at = pl.multiple_of(plane * depth + half * half_rows, half_rows)
         if name.startswith("qkv"):
-            piece = half_rows // 2
+            piece = half_rows // 4
             return wq.at[pl.ds(pl.multiple_of(at + int(name[-1]) * piece, piece), piece), :]
         if name == "out":
             return wo.at[2 * plane + half]
         if name.startswith("down"):
-            piece = hidden_units // 4
-            return wd.at[2 * plane + half, pl.ds(int(name[-1]) * piece, piece)]
+            lanes, part_at = divmod(int(name[-1]), 2)
+            lo = part_at * down_rows
+            return wd.at[
+                2 * plane + half, pl.ds(lo, min(down_rows, hidden_units - lo)), pl.ds(lanes * lane, lane)
+            ]
         ref = wg if name.startswith("gate") else wu
         if name.endswith("0"):
             return ref.at[pl.ds(at, half_rows), pl.ds(0, cut)]
@@ -272,7 +284,7 @@
         ref = region(name, plane, half)
         index = PARTS.index(name) * len(KINDS) + KINDS.index(kind)
         return pltpu.make_async_remote_copy(
-            src_ref=ref, dst_ref=ref, send_sem=w_send.at[index], recv_sem=w_recv.at[index],
+            src_ref=ref, dst_ref=ref, send_sem=w_send.at[KINDS.index(kind)], recv_sem=w_recv.at[index],
             device_id=device, device_id_type=MESH_ID,
         )
 
@@ -281,9 +293,23 @@
     def act_copy(key, src, dst, device):
         index = act_ids.setdefault(key, len(act_ids))
         return pltpu.make_async_remote_copy(
-            src_ref=src, dst_ref=dst, send_sem=a_send.at[index], recv_sem=a_recv.at[index],
-            device_id=device, device_id_type=MESH_ID,
+            src_ref=src, dst_ref=dst, send_sem=a_send.at[GROUPS[key if isinstance(key, str) else key[0]]],
+            recv_sem=a_recv.at[index], device_id=device, device_id_type=MESH_ID,
         )
+
+    def drain(sem, elements):
+        assert elements % wq.shape[1] == 0
+        ref = wq.at[pl.ds(0, elements // wq.shape[1]), :]
+        pltpu.make_async_remote_copy(
+            src_ref=ref, dst_ref=ref, send_sem=sem, recv_sem=a_recv.at[0], device_id={"tp": core},
+            device_id_type=MESH_ID,
+        ).wait_send()
+
+    def drain_weights(sent):
+        for kind in KINDS:
+            total = sum(math.prod(ref.shape) for name, ref in sent if name == kind)
+            if total:
+                drain(w_send.at[KINDS.index(kind)], total)
 
     at_z = pl.multiple_of(z * depth, depth)
     loads = {}
@@ -304,42 +330,50 @@
     load("u", w_up, wu.at[pl.ds(at_z, depth), :])
     load("d0", w_down.at[:, pl.ds(0, block)], wd.at[2 * z])
     load("d1", w_down.at[:, pl.ds(block, block)], wd.at[2 * z + 1])
-    pl.semaphore_wait(barrier, 5)
+    pl.semaphore_wait(barrier, 6)
     for name in ("q", "k", "v"):
         loads[name].wait()
 
     tok_copy = act_copy("tok", tok.at[0], tok.at[1], {"fs": pair_z})
     shift_copy = act_copy("shift", shift_sent.at[0], shift_sent.at[1], {"fs": pair_z})
 
-    out_order = [
-        (2 * zc, None), (2 * zc + 1, None),
-        (2 * zo + r, ("mid_own", zo, r)), (2 * ze + r, ("end_a", ze, r)),
-        (2 * zo + other_r, ("rep_own", zo, other_r)), (2 * zf + r, ("mid_end", zf, r)),
-        (2 * ze + other_r, ("end_b", ze, other_r)), (2 * zf + other_r, ("rep_end", zf, other_r)),
+    out_units = [
+        (2 * zc, None, 0, block, ()), (2 * zc + 1, None, 0, block, ()),
+        (2 * zo + r, ("mid_own", zo, r), 0, block, DOWN), (2 * ze + r, ("end_a", ze, r), 0, block, DOWN),
+        (2 * zf + r, ("mid_end", zf, r), 0, block, DOWN),
+        (2 * ze + other_r, ("end_b", ze, other_r), 0, lane, DOWN[:2]),
+        (2 * zf + other_r, ("rep_end", zf, other_r), 0, lane, DOWN[:2]),
+        (2 * zo + other_r, ("rep_own", zo, other_r), 0, block, DOWN),
+        (2 * ze + other_r, ("end_b", ze, other_r), lane, lane, DOWN[2:]),
+        (2 * zf + other_r, ("rep_end", zf, other_r), lane, lane, DOWN[2:]),
     ]
     mixed_copy = act_copy("mixed", mixed_home, mixed_home, {"fs": pair_z})
-    home_copies = [
-        act_copy(("home", i), ffn_home.at[b], ffn_home.at[b], {"fs": pair_z})
-        for i, (b, _) in enumerate(out_order)
-    ]
+    def home_copy(i, which):
+        b, _, lo, size, _ = out_units[i]
+        lanes = pl.ds(lo, size)
+        src = part.at[b, chip, 1, :, lanes] if which else ffn_home.at[0, b, :, lanes]
+        device = {"fs": pair_z, "tp": chip} if which else {"fs": pair_z}
+        return act_copy(("home", i, which), src, ffn_home.at[which, b, :, lanes], device)
+
+    home_near = [home_copy(i, 0) for i in range(len(out_units))]
+    home_far = [home_copy(i, 1) for i in range(len(out_units))]
 
     @pl.when(jnp.logical_not(is_centre))
     def _():
         sent = []
 
         def send(name, kind, half):
-            copy = weight_copy(name, kind, z, half, {"fs": pair_z})
-            copy.start()
-            sent.append(copy)
-
-        send("qkv0", "end_a", r)
-        send("qkv1", "end_a", r)
+            weight_copy(name, kind, z, half, {"fs": pair_z}).start()
+            sent.append((kind, region(name, z, half)))
+
+        for name in QKV:
+            send(name, "end_a", r)
         loads["o0"].wait()
         loads["o1"].wait()
         send("out", "end_a", r)
         loads["tok"].wait()
         tok_copy.start()
-        send("qkv0", "end_b", other_r)
+        send(QKV[0], "end_b", other_r)
         loads["shift"].wait()
         shift_sent[0] = shift[0].astype(BF16)
         shift_copy.start()
@@ -355,14 +389,18 @@
         for name in DOWN:
             send(name, "end_b", other_r)
         mixed_copy.wait_recv()
-        for i, (b, _) in enumerate(out_order):
-            home_copies[i].wait_recv()
-            cols = pl.ds(pl.multiple_of(b * block, block), block)
-            out[:, cols] = mixed_home[b].astype(F32) + ffn_home[b].astype(F32)
+        for i, (b, _, lo, size, _) in enumerate(out_units):
+            home_near[i].wait_recv()
+            home_far[i].wait_recv()
+            lanes = pl.ds(lo, size)
+            cols = pl.ds(pl.multiple_of(b * block + lo, lane), size)
+            out[:, cols] = (
+                mixed_home[b, :, lanes].astype(F32)
+                + ffn_home[0, b, :, lanes].astype(F32) + ffn_home[1, b, :, lanes].astype(F32)
+            )
         tok_copy.wait_send()
         shift_copy.wait_send()
-        for copy in sent:
-            copy.wait_send()
+        drain_weights(sent)
 
     @pl.when(is_centre)
     def _():
@@ -376,9 +414,8 @@
                 weight_copy(name, kind, plane, half, {"fs": pair_z}).wait_recv()
 
         def send(name, kind, plane, half, device):
-            copy = weight_copy(name, kind, plane, half, device)
-            copy.start()
-            sent.append(copy)
+            weight_copy(name, kind, plane, half, device).start()
+            sent.append((kind, region(name, plane, half)))
 
         def mid_own(*parts):
             for name in parts:
@@ -448,12 +485,7 @@
                 self.from_core.wait_recv()
                 self.passed.wait_recv()
 
-            def drain(self):
-                self.to_chip.wait_send()
-                self.to_core.wait_send()
-                self.pass_on.wait_send()
-
-        mid_own("qkv0", "qkv1")
+        mid_own(*QKV)
         loads["tok"].wait()
         norm_rows(lambda at: tok[0, at, :].astype(F32), mix_gain, x_mix, 0)
         mix_gather = [Gather("mix", x_mix, s) for s in range(2)]
@@ -464,8 +496,8 @@
         bias = decay_bias[:, pl.ds(pl.multiple_of(t * key_cols, key_cols), key_cols)]
         up_cols = w_decay_up[:, pl.ds(pl.multiple_of(t * key_cols, key_cols), key_cols)]
 
-        def project(s):
-            @pl.loop(0, seq // 256)
+        def project(s, lo, hi):
+            @pl.loop(lo, hi)
             def _(i):
                 at = pl.ds(pl.multiple_of(i * 256, 256), 256)
                 x = x_mix[s, at, :]
@@ -575,75 +607,99 @@
                     up = jnp.dot(x, wu[:, cols], preferred_element_type=F32)
                     act[s, at, cols] = (gate / (1.0 + jnp.exp(-gate)) * up).astype(BF16)
 
-        def piece_copies(i, b):
+        def piece_copies(i):
+            b, _, lo, size, _ = out_units[i]
+            lanes = pl.ds(lo, size)
             return (
-                act_copy(("piece", i, 0), part.at[b, core], near2.at[i, 0], {"tp": core}),
-                act_copy(("piece", i, 1), part.at[b, both], near2.at[i, 1], {"tp": core}),
-                act_copy(("piece", i, 2), part.at[b, chip], far2.at[i], {"tp": chip}),
+                act_copy(("piece", i, 0), part.at[b, core, :, :, lanes], near2.at[b, 0, :, :, lanes], {"tp": core}),
+                act_copy(("piece", i, 1), part.at[b, both, :, :, lanes], near2.at[b, 1, :, :, lanes], {"tp": core}),
+                act_copy(("piece", i, 2), part.at[b, chip, 0, :, lanes], far2.at[b, :, lanes], {"tp": chip}),
             )
 
-        pieces = [piece_copies(i, b) for i, (b, _) in enumerate(out_order)]
+        pieces = [piece_copies(i) for i in range(len(out_units))]
 
         def reduce_start(s):
             reduce[s][1].start()
             reduce[s][0].start()
 
         def reduce_drain():
+            drain(a_send.at[3], 6 * rows * width)
+
+        begun = []
+
+        def piece_early(i):
+            b, source, lo, size, chunks = out_units[i]
+            incoming(chunks[0], *source)
             for s in range(2):
-                for copy in reduce[s]:
-                    copy.wait_send()
+                early[len(begun), s] = jnp.dot(
+                    act[s, :, :down_rows], wd[b, :down_rows, lo : lo + size], preferred_element_type=F32
+                )
+            begun.append(i)
 
         def piece_dot(i):
-            b, source = out_order[i]
-            if source is not None:
-                for name in DOWN:
-                    incoming(name, *source)
+            b, source, lo, size, chunks = out_units[i]
+            for name in chunks:
+                incoming(name, *source)
+            lanes = pl.ds(lo, size)
             for s in range(2):
-                value = jnp.dot(act[s], wd[b], preferred_element_type=F32).astype(BF16)
+                if i in begun:
+                    value = early[begun.index(i), s] + jnp.dot(
+                        act[s, :, down_rows:], wd[b, down_rows:, lo : lo + size], preferred_element_type=F32
+                    )
+                else:
+                    value = jnp.dot(act[s], wd[b, :, lo : lo + size], preferred_element_type=F32)
+                value = value.astype(BF16)
                 for k in range(4):
-                    part[b, k, s] = value[k * rows : (k + 1) * rows]
+                    part[b, k, s, :, lanes] = value[k * rows : (k + 1) * rows]
             pieces[i][1].start()
             pieces[i][0].start()
 
         def piece_far(i):
-            b = out_order[i][0]
+            b, _, lo, size, _ = out_units[i]
+            lanes = pl.ds(lo, size)
             pieces[i][1].wait_recv()
-            part[b, chip] = (part[b, chip].astype(F32) + near2[i, 1].astype(F32)).astype(BF16)
-            pieces[i][2].start()
+            for k, copy in ((1, home_far[i]), (0, pieces[i][2])):
+                total = part[b, chip, k, :, lanes].astype(F32) + near2[b, 1, k, :, lanes].astype(F32)
+                part[b, chip, k, :, lanes] = total.astype(BF16)
+                copy.start()
+            pieces[i][0].wait_recv()
+            total = part[b, t, 1, :, lanes].astype(F32) + near2[b, 0, 1, :, lanes].astype(F32)
+            ffn_home[0, b, :, lanes] = total.astype(BF16)
+            home_near[i].start()
 
         def piece_end(i):
-            b = out_order[i][0]
-            pieces[i][0].wait_recv()
+            b, _, lo, size, _ = out_units[i]
+            lanes = pl.ds(lo, size)
             pieces[i][2].wait_recv()
-            total = part[b, t].astype(F32) + near2[i, 0].astype(F32) + far2[i].astype(F32)
-            cols = pl.ds(pl.multiple_of(b * block, block), block)
-            ffn_home[b] = total[1].astype(BF16)
-            home_copies[i].start()
-            out[:, cols] = out[:, cols] + total[0]
+            cols = pl.ds(pl.multiple_of(b * block + lo, lane), size)
+            total = (
+                part[b, t, 0, :, lanes].astype(F32) + near2[b, 0, 0, :, lanes].astype(F32)
+                + far2[b, :, lanes].astype(F32)
+            )
+            out[:, cols] = out[:, cols] + total
 
         n_blk = seq // BLK
-        mid_end("qkv0")
-        rep_own("qkv0")
-        mid_end("qkv1")
-        rep_own("qkv1")
-        rep_end_b("qkv1")
+        for name in QKV:
+            mid_end(name)
+            rep_own(name)
+        rep_end_b(*QKV[1:])
         mid_own("out")
         mix_gather[0].forward()
         mid_end("out")
         mid_own("gate0", "up0")
-        rep_end("qkv0")
-        rep_end("qkv1")
+        rep_end(*QKV)
         rep_own("out")
         mix_gather[0].finish()
         tok_copy.wait_recv()
         norm_rows(lambda at: tok[1, at, :].astype(F32), mix_gain, x_mix, 1)
         mix_gather[1].start()
         rep_end("out")
-        mid_own("gate1")
-        complete("qkv0", "qkv1")
-        project(0)
-        attend(0, 0, n_blk // 2)
+        mid_own("gate1", "up1")
+        complete(*QKV)
+        project(0, 0, seq // 256)
+        attend(0, 0, n_blk // 4)
         rep_own("gate0")
+        attend(0, n_blk // 4, n_blk // 2)
         mix_gather[1].forward()
         attend(0, n_blk // 2, n_blk)
         complete("out")
@@ -651,9 +707,10 @@
         reduce_start(0)
         mix_gather[1].finish()
         shift_copy.wait_recv()
-        project(1)
+        project(1, 0, seq // 512)
         reduce_far(0)
         rep_own("up0")
+        project(1, seq // 512, seq // 256)
         attend(1, 0, n_blk // 2)
         mid_end("gate0")
         rep_own("gate1")
@@ -661,16 +718,15 @@
         mix_out(1)
         reduce_start(1)
         mid_end("up0")
-        mid_own("up1")
         reduce_far(1)
-        rep_end("gate0")
+        rep_own("up1")
         reduce_end(0)
         mid_end("gate1")
+        rep_end("gate0")
+        mid_end("up1")
+        mid_own(*DOWN)
+        reduce_end(1)
         rep_end("up0")
-        mid_end("up1")
-        reduce_end(1)
-        mid_own(*DOWN)
-        rep_own("up1")
         ffn_gather[0].forward()
         rep_end("gate1")
         complete("gate0", "up0")
@@ -683,10 +739,9 @@
         expand(1, 0, cut)
         rep_own("down1")
         complete("gate1", "up1")
+        expand(0, cut, hidden_units)
+        mid_end("down0")
         rep_own("down2")
-        expand(0, cut, hidden_units)
-        rep_own("down3")
-        mid_end("down0")
         expand(1, cut, hidden_units)
         mid_end("down1")
         reduce_drain()
@@ -698,38 +753,40 @@
         piece_dot(2)
         piece_far(1)
         mid_end("down3")
+        mid_own_b("down3")
         piece_dot(3)
         piece_far(2)
+        rep_end("down1")
+        piece_far(3)
+        rep_end("down2")
         piece_end(0)
-        rep_end("down1")
+        piece_end(1)
+        piece_dot(5)
+        rep_end("down3")
         piece_dot(4)
-        piece_far(3)
-        piece_end(1)
-        rep_end("down2")
+        piece_far(5)
+        piece_dot(6)
         piece_far(4)
         piece_end(2)
-        rep_end("down3")
-        piece_dot(5)
         piece_end(3)
-        piece_far(5)
+        piece_far(6)
+        piece_dot(7)
+        piece_early(8)
+        piece_far(7)
+        piece_early(9)
+        piece_end(5)
+        piece_dot(8)
+        piece_dot(9)
+        piece_far(8)
+        piece_far(9)
         piece_end(4)
-        piece_dot(6)
-        piece_far(6)
-        piece_end(5)
-        piece_dot(7)
-        piece_far(7)
         piece_end(6)
         piece_end(7)
-        for gather in mix_gather + ffn_gather:
-            gather.drain()
-        for copies in pieces:
-            for copy in copies:
-                copy.wait_send()
-        mixed_copy.wait_send()
-        for copy in home_copies:
-            copy.wait_send()
-        for copy in sent:
-            copy.wait_send()
+        piece_end(8)
+        piece_end(9)
+        for group, units in ((0, 6), (1, 6), (2, 8)):
+            drain(a_send.at[group], units * rows * width)
+        drain_weights(sent)
 
 
 def per_device_kernel(
@@ -753,7 +810,7 @@
     )
     delta = pl.pallas_call(
         layer_kernel,
-        out_shape=jax.ShapeDtypeStruct((rows, width), F32),
+        out_shape=pltpu.VMEM((rows, width), F32),
         in_specs=[any_spec if i in large else vmem_spec for i in range(len(args))],
         out_specs=vmem_spec,
         scratch_shapes=[
@@ -772,21 +829,22 @@
             pltpu.VMEM((2, 2, blocks, rows, block), BF16),
             pltpu.VMEM((2, blocks, rows, block), BF16),
             pltpu.VMEM((blocks, 2, 2, rows, block), BF16),
-            pltpu.VMEM((blocks, 2, rows, block), BF16),
+            pltpu.VMEM((blocks, rows, block), BF16),
             pltpu.VMEM((2, seq, hidden_units), BF16),
             pltpu.VMEM((2, rows, width), F32),
             pltpu.VMEM((blocks, rows, block), BF16),
-            pltpu.VMEM((blocks, rows, block), BF16),
+            pltpu.VMEM((2, blocks, rows, block), BF16),
             pltpu.VMEM((key_cols // KEY_CHANNELS, DV, KEY_CHANNELS), F32),
             pltpu.VMEM((2, seq, key_cols), BF16),
-            pltpu.SemaphoreType.DMA((16,)),
+            pltpu.VMEM((2, 2, seq, block // 2), F32),
+            pltpu.SemaphoreType.DMA((11,)),
+            pltpu.SemaphoreType.DMA((len(KINDS),)),
             pltpu.SemaphoreType.DMA((len(PARTS) * len(KINDS),)),
-            pltpu.SemaphoreType.DMA((len(PARTS) * len(KINDS),)),
-            pltpu.SemaphoreType.DMA((64,)),
-            pltpu.SemaphoreType.DMA((64,)),
+            pltpu.SemaphoreType.DMA((6,)),
+            pltpu.SemaphoreType.DMA((71,)),
         ],
         compiler_params=pltpu.CompilerParams(
-            collective_id=0, has_side_effects=True, vmem_limit_bytes=67043328
+            collective_id=0, has_side_effects=True, vmem_limit_bytes=65000000
         ),
     )(*args)
     return tokens.astype(F32) + delta

time: 164 us -> 156 us (0.951)
  Pallas kernels: 162 us -> 154 us
    pallas_call x1, Pallas kernels: 162 us -> 154 us  [per_device_kernel(): pl.pallas_call(layer_kernel, out_shape=pltpu.VMEM((rows, width), F32), in...]
where the time goes in v4:
time: 156 us; the launch traced here: 155 us
  Pallas kernels  154 us (99%)
    pallas_call x1, Pallas kernels, per_device_kernel(): pl.pallas_call(layer_kernel, out_shape=pltpu.VMEM((rows, width), F32), in...  154 us

profile of v4, /device:TPU:0, one launch (start us, length us, event | category | flops | bytes accessed | tf_op | source)
XLA Modules:
  0.0 155.4 jit_solution(2101402471019579117)
XLA Ops:
  0.0 0.0 copy-start
  0.0 154.3 %shard_map.145 = f32[128,2048]{1,0:T(8,128)S(1)} custom-call(bf16[128,2048]{1,0:T(8,128)(2,1)} %tokens.1, f32[1,2048]{1,0:T(1,128)} %bitcast.6, bf16[512,256]{1,0:T(8,128)(2,1)} %w_query.1, bf16[512,256]{1,0:T(8,128)(2,1)} %w_key.1, bf16[512,512]{1,0:T(8,128)(2,1)} %w_value.1, bf16[32,2048]{1,0:T(8,128)(2,1)} %bitcast.5, bf16[32,1024]{1,0:T(8,128)(2,1)} %w_decay_up.1, ...), custom_call_target="tpu_custom_call" | custom-call | tf_op jit(solution)/shard_map/pallas_call | solution.py:811
  154.3 0.0 copy-done
  154.3 1.1 convert_add_fusion
Async XLA Ops:
  0.0 154.3 %copy-start = (bf16[128,2048]{1,0:T(8,128)(2,1)S(1)}, bf16[128,2048]{1,0:T(8,128)(2,1)}, u32[]{:S(2)}) copy-start(bf16[128,2048]{1,0:T(8,128)(2,1)} %tokens.1) | copy-start | bytes 1572868
